TPU v7x, 256 devices: a 4x2x16 block of a 4x16x16 slice. The times are simulated.
256 devices in a mesh: grp: 2 (over y), ep: 32 (over z, core), tp: 4 (over x).
Axes of the slice: x: 4, y: 2, z: 16, core: 2. Of those that a mesh axis runs over, the one named last changes fastest.
The devices are a block of a 4x16x16 slice.
Arguments:
- hidden_in: bfloat16 [32768, 2048], P(('grp', 'ep', 'tp')), parts along dimension 0, may hold values from -6 to 6
- expert_ids: int32 [32768, 2], P(('grp', 'ep', 'tp')), parts along dimension 0, may hold values from 0 to 127, all different within a row; in each aligned block of 128 rows (0 to 127, 128 to 255, ...) at most 4 rows name the same one
- route_weights: float32 [32768, 2], P(('grp', 'ep', 'tp')), parts along dimension 0, may hold values from 0.1 to 1
- norm_gain: float32 [2048], replicated, may hold values from 0.1 to 1.9
- gate_proj: bfloat16 [128, 2048, 512], P(('ep', 'tp')), may hold values from -0.125 to 0.125
- up_proj: bfloat16 [128, 2048, 512], P(('ep', 'tp')), may hold values from -0.125 to 0.125
- down_proj: bfloat16 [128, 512, 2048], P(('ep', 'tp')), may hold values from -0.25 to 0.25
Outputs:
- mixed_out: bfloat16 [32768, 2048], P(('grp', 'ep', 'tp')), parts along dimension 0
There are 2 independent parts, one for each index of `grp`. A program takes and returns all parts, laid end to end along the dimension named above; an argument that names none is the same for every part. Nothing has to cross between parts.
Inputs may be any that keep to these rules, and one draw needn't show every extreme that they name: `expert_ids`: each token names 2 different experts; among the 128 tokens of one device (aligned blocks of rows) no expert is named more than 4 times, and in every draw some expert is named exactly 4 times by some device's tokens.
All inputs are finite; a program needn't handle non-finite values.
Results may differ from a plain program's by a relative error of at most 0.0071.
Values may be sent and summed in bfloat16 or wider, within the bound.
A program may use at most 64 MiB of HBM per device.

v0:
```python
import jax
import jax.numpy as jnp
from jax import lax
from jax.sharding import PartitionSpec as P


def body(hidden_in, expert_ids, route_weights, norm_gain, gate_proj, up_proj, down_proj):
    token_count = hidden_in.shape[0]
    model_width = hidden_in.shape[1]
    choose_count = expert_ids.shape[1]
    ep_count = lax.axis_size("ep")
    tp_count = lax.axis_size("tp")
    expert_count = ep_count * tp_count
    capacity = max(2, 2 * choose_count * token_count // expert_count)
    as_float = hidden_in.astype(jnp.float32)
    scaled = as_float * lax.rsqrt(jnp.mean(as_float * as_float, axis=-1, keepdims=True) + 1e-06)
    normed = (scaled * norm_gain).astype(jnp.bfloat16)
    flat_ids = expert_ids.reshape(-1)
    onehot = (flat_ids[:, None] == jnp.arange(expert_count, dtype=jnp.int32)[None, :]).astype(
        jnp.int32
    )
    slot_index = jnp.sum((jnp.cumsum(onehot, axis=0) - onehot) * onehot, axis=1)
    target = flat_ids * capacity + slot_index
    routed = jnp.repeat(normed, choose_count, axis=0)
    buffer = jnp.zeros((expert_count * capacity, model_width), jnp.bfloat16).at[target].set(routed)
    buffer = buffer.reshape(expert_count, capacity, model_width)
    arrived = lax.all_to_all(buffer, ("ep", "tp"), split_axis=0, concat_axis=0, tiled=True)
    shape_in = arrived.shape
    block_in = arrived.reshape(-1, model_width)
    gate_act = jnp.dot(block_in, gate_proj[0], preferred_element_type=jnp.float32)
    up_act = jnp.dot(block_in, up_proj[0], preferred_element_type=jnp.float32)
    hidden = (jax.nn.silu(gate_act) * up_act).astype(jnp.bfloat16)
    result = jnp.dot(hidden, down_proj[0], preferred_element_type=jnp.float32).astype(jnp.bfloat16)
    results = result.reshape(shape_in)
    returned = lax.all_to_all(results, ("ep", "tp"), split_axis=0, concat_axis=0, tiled=True)
    picked = returned.reshape(-1, model_width)[target].astype(jnp.float32)
    picked = picked.reshape(token_count, choose_count, model_width)
    return jnp.sum(picked * route_weights[:, :, None], axis=1).astype(jnp.bfloat16)


def solution(mesh):
    return jax.shard_map(
        body,
        mesh=mesh,
        in_specs=(
            P(("grp", "ep", "tp"), None),
            P(("grp", "ep", "tp"), None),
            P(("grp", "ep", "tp"), None),
            P(),
            P(("ep", "tp"), None, None),
            P(("ep", "tp"), None, None),
            P(("ep", "tp"), None, None),
        ),
        out_specs=P(("grp", "ep", "tp"), None),
        check_vma=False,
    )
```

profile of v0, /device:TPU:33, one launch (start us, length us, event | category | flops | bytes accessed | tf_op | source)
XLA Modules:
  0.0 286.3 jit_solution(2377975714317678964)
XLA Ops:
  0.0 0.9 copy.10
  0.9 0.1 eq.29
  1.1 0.1 eq.25
  1.2 0.7 broadcast_multiply_fusion
  2.0 0.2 fusion.19
  2.4 0.1 mul.55
  2.6 1.2 fusion.11
  3.8 1.2 fusion.13
  5.1 0.6 broadcast_in_dim.5
  5.7 1.2 reshape.94
  6.9 0.2 fusion.21
  7.1 4.4 %scatter_custom_fusion = bf16[512,2048]{1,0:T(8,128)(2,1)} fusion(s32[256]{0:T(256)S(1)} %bitcast.36, bf16[256,2048]{1,0:T(8,128)(2,1)} %reshape.94, bf16[]{:T(256)} %constant.8.clone.1), kind=kCustom, calls=%fused_computation.16 | custom fusion | bytes 2097664 | tf_op jit(solution)/shard_map/scatter | solution.py:25
  11.6 4.1 %reshape.77 = bf16[128,4,2048]{2,1,0:T(4,128)(2,1)} reshape(bf16[512,2048]{1,0:T(8,128)(2,1)} %scatter_custom_fusion) | data formatting | bytes 4194304 | tf_op jit(solution)/shard_map/reshape | solution.py:26
  15.7 129.0 %all_to_all.10 = bf16[128,4,2048]{2,1,0:T(4,128)(2,1)} all-to-all(bf16[128,4,2048]{2,1,0:T(4,128)(2,1)} %reshape.77), channel_id=1, replica_groups=mesh['grp'=2,'ep'=32,'tp'=4] {'ep','tp'}, dimensions={0} | all-to-all | bytes 4194304 | tf_op jit(solution)/shard_map/all_to_all | solution.py:27
  144.7 4.0 %reshape.78 = bf16[512,2048]{1,0:T(8,128)(2,1)} reshape(bf16[128,4,2048]{2,1,0:T(4,128)(2,1)} %all_to_all.10) | data formatting | bytes 4194304 | tf_op jit(solution)/shard_map/reshape | solution.py:29
  148.6 3.5 %fusion.3 = f32[512,512]{1,0:T(8,128)S(1)} fusion(bf16[512,2048]{1,0:T(8,128)(2,1)} %reshape.78, bf16[1,2048,512]{2,1,0:T(8,128)(2,1)} %param.11), kind=kOutput, calls=%fused_computation.6 | convolution fusion | flops 1073741824 | bytes 5242880 | tf_op jit(solution)/shard_map/dot_general | solution.py:30
  152.1 6.0 %convolution_convert_fusion = bf16[512,2048]{1,0:T(8,128)(2,1)} fusion(bf16[1,512,2048]{2,1,0:T(8,128)(2,1)S(1)} %copy-done, bf16[512,2048]{1,0:T(8,128)(2,1)} %reshape.78, bf16[1,2048,512]{2,1,0:T(8,128)(2,1)} %param.12, f32[512,512]{1,0:T(8,128)S(1)} %fusion.3), kind=kOutput, calls=%fused_computation.2 | convolution fusion | flops 2150105088 | bytes 9437184 | tf_op jit(solution)/shard_map/dot_general | solution.py:33
  158.1 4.1 %reshape.79 = bf16[128,4,2048]{2,1,0:T(4,128)(2,1)} reshape(bf16[512,2048]{1,0:T(8,128)(2,1)} %convolution_convert_fusion) | data formatting | bytes 4194304 | tf_op jit(solution)/shard_map/reshape | solution.py:34
  162.3 10.0 %all-to-all-start.1 = ((bf16[128,4,2048]{2,1,0:T(4,128)(2,1)}), bf16[128,4,2048]{2,1,0:T(4,128)(2,1)}, u32[]{:S(2)}, u32[]{:S(2)}) async-start(bf16[128,4,2048]{2,1,0:T(4,128)(2,1)} %reshape.79), calls=%async_computation.1 | async-start | bytes 4194304 | tf_op jit(solution)/shard_map/all_to_all | solution.py:35
  172.4 97.8 %all-to-all-done.1 = bf16[128,4,2048]{2,1,0:T(4,128)(2,1)} async-done(((bf16[128,4,2048]{2,1,0:T(4,128)(2,1)}), bf16[128,4,2048]{2,1,0:T(4,128)(2,1)}, u32[]{:S(2)}, u32[]{:S(2)}) %all-to-all-start.1) | async-done | bytes 2097184 | tf_op jit(solution)/shard_map/all_to_all | solution.py:35
  270.2 4.0 %reshape.80 = bf16[512,2048]{1,0:T(8,128)(2,1)} reshape(bf16[128,4,2048]{2,1,0:T(4,128)(2,1)} %all-to-all-done.1) | data formatting | bytes 4194304 | tf_op jit(solution)/shard_map/reshape | solution.py:36
  274.1 4.2 %gather_fusion = bf16[256,2048]{1,0:T(8,128)(2,1)S(1)} fusion(bf16[512,2048]{1,0:T(8,128)(2,1)} %reshape.80, s32[1024]{0:T(1024)S(1)} %pad_clamp_fusion), kind=kCustom, calls=%fused_computation | custom fusion | bytes 2098176 | tf_op jit(solution)/shard_map/gather | solution.py:36
  278.4 2.4 reshape.81
  280.7 5.6 %multiply_reduce_fusion = bf16[128,2048]{1,0:T(8,128)(2,1)} fusion(f32[128,2,2048]{2,1,0:T(2,128)} %reshape.81, f32[128,2]{1,0:T(8,128)S(1)} %copy.14), kind=kLoop, calls=%fused_computation.8 | loop fusion | flops 786432 | bytes 2622464 | tf_op jit(solution)/shard_map/reduce_sum | solution.py:38
  (16 shorter events, 0.4 us)
Async XLA Ops:
  0.0 152.1 %copy-start = (bf16[1,512,2048]{2,1,0:T(8,128)(2,1)S(1)}, bf16[1,512,2048]{2,1,0:T(8,128)(2,1)}, u32[]{:S(2)}) copy-start(bf16[1,512,2048]{2,1,0:T(8,128)(2,1)} %param.13) | copy-start | bytes 6291460
  162.3 10.0 %copy-start.1 = (f32[128,2]{0,1:T(2,128)S(1)}, f32[128,2]{0,1:T(2,128)}, u32[]{:S(2)}) copy-start(f32[128,2]{0,1:T(2,128)} %param.9) | copy-start | bytes 3076
  162.3 107.9 %all-to-all-start.1 = ((bf16[128,4,2048]{2,1,0:T(4,128)(2,1)}), bf16[128,4,2048]{2,1,0:T(4,128)(2,1)}, u32[]{:S(2)}, u32[]{:S(2)}) async-start(bf16[128,4,2048]{2,1,0:T(4,128)(2,1)} %reshape.79), calls=%async_computation.1 | async-start | bytes 4194304 | tf_op jit(solution)/shard_map/all_to_all | solution.py:35
where the time goes:
time: 287 us; the launch traced here: 286 us
  blocking collectives  129 us (45%)
  waiting for transfers between devices  97.8 us (34%)
  local copies, waits for them, and re-layouts  30.8 us (11%)
  starting transfers between devices  10 us (3%)
  matrix products  9.49 us (3%)
  other arithmetic  9.19 us (3%)
    all_to_all x1, blocking collectives, body(): lax.all_to_all(buffer, ('ep', 'tp'), split_axis=0, concat_axis=0, tiled=T...  129 us
    all_to_all x1, waiting for transfers between devices, body(): lax.all_to_all(results, ('ep', 'tp'), split_axis=0, concat_axis=0, tiled=...  97.8 us
    all_to_all x1, starting transfers between devices, body(): lax.all_to_all(results, ('ep', 'tp'), split_axis=0, concat_axis=0, tiled=...  10 us
    dot_general x1, matrix products, body(): jnp.dot(hidden, down_proj[0], preferred_element_type=jnp.float32)  6.03 us
  transfers between devices with their start and end apart: 1, of which 1 were waited for; matrix products, arithmetic and copies ran while one was open for 0% of the time, Pallas kernels for 0%

commit v1 on v0

v1 whole, which is shorter than its diff:
```python
import functools

import jax
import jax.numpy as jnp
from jax import lax
from jax.experimental import pallas as pl
from jax.experimental.pallas import tpu as pltpu
from jax.sharding import PartitionSpec as P

MESH = pl.DeviceIdType.MESH
BF = jnp.bfloat16
F32 = jnp.float32
I32 = jnp.int32
Q = 4


def mm(a, b):
    return jnp.dot(a, b, preferred_element_type=F32)


def mm_nt(a, b):
    return lax.dot_general(a, b, (((1,), (1,)), ((), ())), preferred_element_type=F32)


class Dims:
    def __init__(self, ep, tp, tokens, width, fe, cap):
        self.NZ, self.NX = ep // 2, tp
        self.T, self.D, self.FE, self.CAP = tokens, width, fe, cap
        self.DQ = width // Q
        self.H = self.NZ // 2
        self.PL = 2 * tp
        self.RB = Q * cap
        self.NR = self.PL * self.RB
        self.HB = self.H // 2
        self.SR = self.PL * 2 * cap
        plane = self.PL * cap
        self.caps = [tokens] + [
            min(tokens, (self.H - k) * plane + plane // 2) for k in range(1, self.H + 1)
        ]
        packed = [k for k in range(1, self.H + 1) if self.caps[k] < tokens]
        self.KP = packed[0] if packed else self.H + 1


def kernel(
    dm, hid, meta, gain, wg, wu, wd, out,
    xs, metas, zb, zp, rin, rout, stage, rows, ysend, yrecv,
    ex, cm, sm, st, erow, upper, perm_g, perm_s, acc, xb, gacc, uacc, hb, yb,
    wgv, wuv, wdv,
    w_sem, m_send, m_recv, z_send, z_recv, p_send, p_recv, y_send, y_recv, r_send, r_recv,
):
    NZ, NX, T, D, FE, CAP = dm.NZ, dm.NX, dm.T, dm.D, dm.FE, dm.CAP
    DQ, H, PL, RB, NR, HB, SR, KP, caps = dm.DQ, dm.H, dm.PL, dm.RB, dm.NR, dm.HB, dm.SR, dm.KP, dm.caps
    ep, x = lax.axis_index("ep"), lax.axis_index("tp")
    z, c = ep // 2, ep % 2

    def at_z(other):
        return {"ep": other * 2 + c, "tp": x}

    def in_plane(j):
        dc, dx = j // NX, j % NX
        return {"ep": z * 2 + (c + dc) % 2, "tp": (x + dx) % NX}

    def mirror(j):
        return (j // NX) * NX + (NX - j % NX) % NX

    barrier = pltpu.get_barrier_semaphore()
    for d in range(1, NZ):
        pl.semaphore_signal(barrier, inc=1, device_id=at_z((z + d) % NZ), device_id_type=MESH)
    for j in range(1, PL):
        pl.semaphore_signal(barrier, inc=1, device_id=in_plane(j), device_id_type=MESH)

    weight_copies = []
    for q in range(Q):
        weight_copies.append(pltpu.make_async_copy(wg.at[0, pl.ds(q * DQ, DQ)], wgv.at[q], w_sem.at[0, q]))
        weight_copies.append(pltpu.make_async_copy(wu.at[0, pl.ds(q * DQ, DQ)], wuv.at[q], w_sem.at[1, q]))
        weight_copies.append(pltpu.make_async_copy(wd.at[0, :, pl.ds(q * DQ, DQ)], wdv.at[q], w_sem.at[2, q]))
    for copy in weight_copies:
        copy.start()

    NB = 16

    def norm_rows(b, _):
        r = pl.ds(pl.multiple_of(b * NB, NB), NB)
        v = hid[r, :].astype(F32)
        scale = lax.rsqrt(jnp.mean(v * v, axis=-1, keepdims=True) + 1e-06)
        n = ((v * scale) * gain[...]).astype(BF)
        for q in range(Q):
            xs[q, r, :] = n[:, q * DQ:(q + 1) * DQ]
        return 0

    lax.fori_loop(0, T // NB, norm_rows, 0)

    metas[0] = meta[...]
    r_id = lax.broadcasted_iota(I32, (NR, T), 0)
    j_id = r_id // RB
    dx_id, dc_id = j_id % NX, j_id // NX
    erow[...] = z * PL + ((c + dc_id) % 2) * NX + (x + dx_id) % NX
    slot_row = lax.broadcasted_iota(I32, (NR, T), 0) % CAP
    t_row = lax.broadcasted_iota(I32, (T, T), 0)
    t_col = lax.broadcasted_iota(I32, (T, T), 1)
    upper[...] = jnp.where(t_row < t_col, 1.0, 0.0).astype(BF)
    PR = Q * SR
    a_id = lax.broadcasted_iota(I32, (PR, PR), 0)
    n_id = lax.broadcasted_iota(I32, (PR, PR), 1)
    q_of, m_of = a_id // SR, a_id % SR
    perm_g[...] = jnp.where(n_id == (m_of // CAP) * RB + q_of * CAP + m_of % CAP, 1.0, 0.0).astype(BF)
    q_of, m_of = n_id // SR, n_id % SR
    perm_s[...] = jnp.where(a_id == (m_of // CAP) * RB + q_of * CAP + m_of % CAP, 1.0, 0.0).astype(BF)

    pl.semaphore_wait(barrier, NZ - 1 + PL - 1)

    meta_copies = [
        pltpu.make_async_remote_copy(
            src_ref=meta, dst_ref=metas.at[d], send_sem=m_send.at[d], recv_sem=m_recv.at[d],
            device_id=at_z((z + d) % NZ), device_id_type=MESH,
        )
        for d in range(1, NZ)
    ]
    for copy in meta_copies:
        copy.start()

    def z_copy(src, direction, k, q, rows_sent):
        return pltpu.make_async_remote_copy(
            src_ref=src, dst_ref=zb.at[direction, k - 1, q, pl.ds(0, rows_sent)],
            send_sem=z_send.at[direction, k - 1, q], recv_sem=z_recv.at[direction, k - 1, q],
            device_id=at_z((z + 1 - 2 * direction + NZ) % NZ), device_id_type=MESH,
        )

    def send_own(i, _):
        q, direction = i // 2, i % 2
        z_copy(xs.at[q], direction, 1, q, caps[1]).start()
        return 0

    lax.fori_loop(0, 2 * Q, send_own, 0)

    def build(direction, k):
        d = k + direction * (NZ - 2 * k)
        s = (z - d + NZ) % NZ
        m = metas[d]
        ids = [m[i:i + 1, :].astype(I32) for i in range(2)]
        wts = [m[2 + i:3 + i, :] for i in range(2)]
        e = erow[...]
        hit0, hit1 = e == ids[0], e == ids[1]
        hit = jnp.where(hit0, 1.0, 0.0) + jnp.where(hit1, 1.0, 0.0)
        count = mm(hit.astype(BF), upper[...])
        last = jnp.where(k == H, 1, 0)
        other_way = last * jnp.where(e % 2 == direction, 0, 1)
        sel = jnp.where(count == slot_row.astype(F32), hit, 0.0)
        sel = jnp.where(other_way == 1, 0.0, sel)
        pick = sel.astype(BF)
        weighted = ((jnp.where(hit0, wts[0], 0.0) + jnp.where(hit1, wts[1], 0.0)) * sel).astype(BF)

        reach = jnp.zeros((1, T), I32)
        for i in range(2):
            dist = ids[i] // PL - s
            dist = jnp.where(dist < 0, dist + NZ, dist)
            odd = ids[i] % 2
            up_way = jnp.where(dist < H, dist, jnp.where((dist == H) & (odd == 0), H, 0))
            down_way = jnp.where(dist > H, NZ - dist, jnp.where((dist == H) & (odd == 1), H, 0))
            reach = jnp.maximum(reach, jnp.where(direction == 0, up_way, down_way))

        def place(kk):
            mask = jnp.where(reach >= kk, 1.0, 0.0)
            pos = mm(jnp.broadcast_to(mask, (8, T)).astype(BF), upper[...])[0:1, :].astype(I32)
            pos = jnp.where(reach >= kk, pos, -1)
            col = lax.broadcasted_iota(I32, (1, T), 1)
            pos = jnp.where(kk >= KP, pos, col)
            return jnp.where(t_row == pos, 1.0, 0.0).astype(BF)

        here, after = place(k), place(k + 1)
        ex[direction, k] = mm_nt(pick, here).astype(BF)
        cm[direction, k] = mm_nt(here, weighted).astype(BF)
        sm[direction, k] = mm_nt(after, here).astype(BF)
        st[direction, k] = mm_nt(here, after).astype(BF)

    def build_steps(lo, hi):
        def one(i, _):
            build(i % 2, lo + i // 2)
            return 0

        lax.fori_loop(0, 2 * (hi - lo), one, 0)

    q_row = (lax.broadcasted_iota(I32, (NR, 1), 0) // CAP) % Q

    def only_q_rows(v, q):
        return jnp.where(q_row == q, v.astype(F32), 0.0).astype(BF)

    q_col = (lax.broadcasted_iota(I32, (1, NR), 1) // CAP) % Q

    def only_q_cols(v, q):
        return jnp.where(q_col == q, v.astype(F32), 0.0).astype(BF)

    build(0, 0)
    own = jnp.zeros((NR, DQ), F32)
    for q in range(Q):
        own = own + mm(only_q_rows(ex[0, 0], q), xs[q])
    own = own.astype(BF).reshape(PL, RB, DQ)
    stage[H - 1, :, 1] = own
    rows[H - 1, 0, 1] = own[0]

    for copy in meta_copies:
        copy.wait()

    def dispatch(k):
        ck = caps[k]
        acc[...] = jnp.zeros_like(acc)

        def chunk(i, _):
            q, direction = i // 2, i % 2
            z_copy(zb.at[direction, k - 1, q, pl.ds(0, ck)], direction, k, q, ck).wait_recv()
            data = zb[direction, k - 1, q, pl.ds(0, ck), :]
            if k < H:
                cn = caps[k + 1]
                if k + 1 >= KP:
                    p = k + 1 - KP
                    zp[direction, p, q, pl.ds(0, cn), :] = mm(
                        sm[direction, k, pl.ds(0, cn), pl.ds(0, ck)] if ck == T else sm[direction, k][:cn, :ck], data
                    ).astype(BF)
                    source = zp.at[direction, p, q, pl.ds(0, cn)]
                else:
                    source = zb.at[direction, k - 1, q, pl.ds(0, cn)]
                z_copy(source, direction, k + 1, q, cn).start()
            e = only_q_rows(ex[direction, k], q)
            if ck < T:
                e = e[:, :ck]
            block = direction if k < H else 0
            acc[block] = acc[block] + mm(e, data)
            return 0

        lax.fori_loop(0, 2 * Q, chunk, 0)
        for block in range(2 if k < H else 1):
            v = acc[block].astype(BF).reshape(PL, RB, DQ)
            stage[k - 1, :, block] = v
            rows[k - 1, 0, block] = v[0]
        for j in range(1, PL):
            plane_copy(stage, rows, k, j, p_send, p_recv).start()

    def plane_copy(src, dst, k, j, send, recv):
        return pltpu.make_async_remote_copy(
            src_ref=src.at[k - 1, j], dst_ref=dst.at[k - 1, mirror(j)],
            send_sem=send.at[k - 1, j], recv_sem=recv.at[k - 1, mirror(j)],
            device_id=in_plane(j), device_id_type=MESH,
        )

    def plane_wait(src, dst, k, send, recv):
        for j in range(1, PL):
            plane_copy(src, dst, k, mirror(j), send, recv).wait_recv()

    def experts(k0):
        BR = HB * SR
        for i in range(HB):
            k = k0 + i
            plane_wait(stage, rows, k, p_send, p_recv)
            got = mm(perm_g[...], rows[k - 1].reshape(PR, DQ)).astype(BF).reshape(Q, SR, DQ)
            xb[:, pl.ds(i * SR, SR), :] = got
        gacc[...] = jnp.zeros_like(gacc)
        uacc[...] = jnp.zeros_like(uacc)

        def inner(q, _):
            v = xb[q]
            gacc[...] += mm(v, wgv[q])
            uacc[...] += mm(v, wuv[q])
            return 0

        lax.fori_loop(0, Q, inner, 0)
        g = gacc[...]
        hb[...] = ((g / (1.0 + jnp.exp(-g))) * uacc[...]).astype(BF)

        def outer(q, _):
            yb[q] = mm(hb[...], wdv[q]).astype(BF)
            return 0

        lax.fori_loop(0, Q, outer, 0)
        for i in range(HB):
            k = k0 + i
            v = yb[:, pl.ds(i * SR, SR), :].reshape(PR, DQ)
            v = mm(perm_s[...], v).astype(BF).reshape(PL, 2, RB, DQ)
            ysend[k - 1] = v
            yrecv[k - 1, 0] = v[0]
            for j in range(1, PL):
                plane_copy(ysend, yrecv, k, j, y_send, y_recv).start()

    build_steps(1, min(3, H + 1))
    built = min(3, H + 1)
    for k in range(1, H + 1):
        dispatch(k)
        if built <= H:
            nxt = min(built + 2, H + 1)
            build_steps(built, nxt)
            built = nxt
        if k == 1:
            for copy in weight_copies:
                copy.wait()
        if k == HB + 1:
            experts(1)
    experts(HB + 1)

    def r_copy(direction, k, q):
        return pltpu.make_async_remote_copy(
            src_ref=rout.at[direction, k - 1, q, pl.ds(0, caps[k])],
            dst_ref=rin.at[direction, k - 1, q, pl.ds(0, caps[k])],
            send_sem=r_send.at[direction, k - 1, q], recv_sem=r_recv.at[direction, k - 1, q],
            device_id=at_z((z - 1 + 2 * direction + NZ) % NZ), device_id_type=MESH,
        )

    for k in range(H, 0, -1):
        ck = caps[k]
        plane_wait(ysend, yrecv, k, y_send, y_recv)

        def back(i, _, k=k, ck=ck):
            q, direction = i // 2, i % 2
            block = direction if k < H else 0
            y = yrecv[k - 1, :, block].reshape(NR, DQ)
            v = mm(only_q_cols(cm[direction, k, pl.ds(0, ck), :], q), y)
            if k < H:
                cn = caps[k + 1]
                r_copy(direction, k + 1, q).wait_recv()
                far = rin[direction, k, q, pl.ds(0, cn), :]
                if k + 1 >= KP:
                    v = v + mm(st[direction, k][:ck, :cn], far)
                else:
                    v = v + far.astype(F32)
            rout[direction, k - 1, q, pl.ds(0, ck), :] = v.astype(BF)
            r_copy(direction, k, q).start()
            return 0

        lax.fori_loop(0, 2 * Q, back, 0)

    y_own = yrecv[H - 1, :, 1].reshape(NR, DQ)
    for q in range(Q):
        v = mm(only_q_cols(cm[0, 0], q), y_own)
        for direction in range(2):
            r_copy(direction, 1, q).wait_recv()
            v = v + rin[direction, 0, q].astype(F32)
        out[:, q * DQ:(q + 1) * DQ] = v.astype(BF)

    for k in range(1, H + 1):
        def drained(i, _, k=k):
            q, direction = i // 2, i % 2
            z_copy(xs.at[q, pl.ds(0, caps[k])], direction, k, q, caps[k]).wait_send()
            r_copy(direction, k, q).wait_send()
            return 0

        lax.fori_loop(0, 2 * Q, drained, 0)
        for j in range(1, PL):
            plane_copy(stage, rows, k, j, p_send, p_recv).wait_send()
            plane_copy(ysend, yrecv, k, j, y_send, y_recv).wait_send()


def body(hidden_in, expert_ids, route_weights, norm_gain, gate_proj, up_proj, down_proj):
    tokens, width = hidden_in.shape
    chosen = expert_ids.shape[1]
    ep, tp = lax.axis_size("ep"), lax.axis_size("tp")
    fe = gate_proj.shape[2]
    cap = max(2, 2 * chosen * tokens // (ep * tp))
    dm = Dims(ep, tp, tokens, width, fe, cap)
    meta = jnp.concatenate(
        [expert_ids.T.astype(F32), route_weights.T, jnp.zeros((4, tokens), F32)], axis=0
    )
    H, T, DQ, PL, RB, NR, NZ, SR, HB = dm.H, dm.T, dm.DQ, dm.PL, dm.RB, dm.NR, dm.NZ, dm.SR, dm.HB
    vm = pltpu.VMEM
    packed = max(1, H - dm.KP + 1)
    dma = pltpu.SemaphoreType.DMA
    return pl.pallas_call(
        functools.partial(kernel, dm),
        out_shape=jax.ShapeDtypeStruct((tokens, width), BF),
        in_specs=[pl.BlockSpec(memory_space=vm)] * 3 + [pl.BlockSpec(memory_space=pl.ANY)] * 3,
        out_specs=pl.BlockSpec(memory_space=vm),
        scratch_shapes=[
            vm((Q, T, DQ), BF),
            vm((NZ, 8, T), F32),
            vm((2, H, Q, T, DQ), BF),
            vm((2, packed, Q, dm.caps[min(dm.KP, H)], DQ), BF),
            vm((2, H, Q, T, DQ), BF),
            vm((2, H, Q, T, DQ), BF),
            vm((H, PL, 2, RB, DQ), BF),
            vm((H, PL, 2, RB, DQ), BF),
            vm((H, PL, 2, RB, DQ), BF),
            vm((H, PL, 2, RB, DQ), BF),
            vm((2, H + 1, NR, T), BF),
            vm((2, H + 1, T, NR), BF),
            vm((2, H + 1, T, T), BF),
            vm((2, H + 1, T, T), BF),
            vm((NR, T), I32),
            vm((T, T), BF),
            vm((Q * SR, Q * SR), BF),
            vm((Q * SR, Q * SR), BF),
            vm((2, NR, DQ), F32),
            vm((Q, HB * SR, DQ), BF),
            vm((HB * SR, fe), F32),
            vm((HB * SR, fe), F32),
            vm((HB * SR, fe), BF),
            vm((Q, HB * SR, DQ), BF),
            vm((Q, DQ, fe), BF),
            vm((Q, DQ, fe), BF),
            vm((Q, fe, DQ), BF),
            dma((3, Q)),
            dma((NZ,)),
            dma((NZ,)),
            dma((2, H, Q)),
            dma((2, H, Q)),
            dma((H, PL)),
            dma((H, PL)),
            dma((H, PL)),
            dma((H, PL)),
            dma((2, H, Q)),
            dma((2, H, Q)),
        ],
        compiler_params=pltpu.CompilerParams(
            collective_id=0, has_side_effects=True, vmem_limit_bytes=66 * 1000 * 1000
        ),
        name="routed_experts",
    )(hidden_in, meta, norm_gain.reshape(1, width), gate_proj, up_proj, down_proj)


def solution(mesh):
    return jax.shard_map(
        body,
        mesh=mesh,
        in_specs=(
            P(("grp", "ep", "tp"), None),
            P(("grp", "ep", "tp"), None),
            P(("grp", "ep", "tp"), None),
            P(),
            P(("ep", "tp"), None, None),
            P(("ep", "tp"), None, None),
            P(("ep", "tp"), None, None),
        ),
        out_specs=P(("grp", "ep", "tp"), None),
        check_vma=False,
    )
```

time: 287 us -> 212 us (0.74)
  Pallas kernels: 0 us -> 207 us
  blocking collectives: 129 us -> 0 us
  waiting for transfers between devices: 97.8 us -> 0 us
  local copies, waits for them, and re-layouts: 30.8 us -> 1.96 us
  starting transfers between devices: 10 us -> 0 us
  matrix products: 9.49 us -> 0 us
  other arithmetic: 9.19 us -> 2.02 us
    pallas_call x0 -> x1, Pallas kernels: none -> 207 us  [body(): pl.pallas_call(functools.partial(kernel, dm), out_shape=jax.ShapeDtypeStr...]
    all_to_all x1 -> x0, blocking collectives: 129 us -> none  [body(): lax.all_to_all(buffer, ('ep', 'tp'), split_axis=0, concat_axis=0, tiled=T...]
    all_to_all x1 -> x0, waiting for transfers between devices: 97.8 us -> none  [body(): lax.all_to_all(results, ('ep', 'tp'), split_axis=0, concat_axis=0, tiled=...]
    reshape x5 -> x0, local copies, waits for them, and re-layouts: 17.4 us -> none  [the longest x1 4.12 us: body(): buffer = buffer.reshape(expert_count, capacity, model_width)]
    all_to_all x1 -> x0, starting transfers between devices: 10 us -> none  [body(): lax.all_to_all(results, ('ep', 'tp'), split_axis=0, concat_axis=0, tiled=...]
    dot_general x2 -> x0, matrix products: 9.49 us -> none  [the longest x1 6.03 us: body(): jnp.dot(hidden, down_proj[0], preferred_element_type=jnp.float32)]
    reduce_sum x3 -> x0, other arithmetic: 7 us -> none  [the longest x1 5.59 us: body(): jnp.sum(picked * route_weights[:, :, None], axis=1).astype(jnp.bfloat16)]
    scatter x1 -> x0, local copies, waits for them, and re-layouts: 4.43 us -> none  [body(): jnp.zeros((expert_count * capacity, model_width), jnp.bfloat16).at[target]]
  transfers between devices with their start and end apart: 1 -> 0, of which waited for: 1 -> 0; matrix products, arithmetic and copies ran while one was open for 0% -> 0% of each run, Pallas kernels for 0% -> 0%
where the time goes in v1:
time: 212 us; the launch traced here: 211 us
  Pallas kernels  207 us (98%)
    pallas_call x1, Pallas kernels, body(): pl.pallas_call(functools.partial(kernel, dm), out_shape=jax.ShapeDtypeStr...  207 us

profile of v1, /device:TPU:33, one launch (start us, length us, event | category | flops | bytes accessed | tf_op | source)
XLA Modules:
  0.0 211.2 jit_solution(8364102264327897165)
XLA Ops:
  0.0 0.1 pad.2.clone
  0.1 0.7 convert_bitcast_fusion
  0.8 1.3 maximum_maximum_fusion.meta
  2.1 207.2 %routed_experts.1 = bf16[128,2048]{1,0:T(8,128)(2,1)} custom-call(bf16[128,2048]{1,0:T(8,128)(2,1)} %hid.1, f32[8,128]{1,0:T(8,128)} %maximum_maximum_fusion.meta, f32[1,2048]{1,0:T(1,128)} %bitcast.4, bf16[1,2048,512]{2,1,0:T(8,128)(2,1)} %wg.1, bf16[1,2048,512]{2,1,0:T(8,128)(2,1)} %wu.1, bf16[1,512,2048]{2,1,0:T(8,128)(2,1)} %wd.1), custom_call_target="tpu_custom_call" | custom-call | tf_op jit(solution)/shard_map/routed_experts/pallas_call | solution.py:364
  209.3 1.9 copy.9
  (1 shorter events, 0.0 us)

commit v2 on v1

--- a/solution.py
+++ b/solution.py
@@ -31,7 +31,6 @@
         self.PL = 2 * tp
         self.RB = Q * cap
         self.NR = self.PL * self.RB
-        self.HB = self.H // 2
         self.SR = self.PL * 2 * cap
         plane = self.PL * cap
         self.caps = [tokens] + [
@@ -42,19 +41,25 @@
 
 
 def kernel(
-    dm, hid, meta, gain, wg, wu, wd, out,
+    dm, hid, ids_in, wts_in, gain, wg, wu, wd, out,
     xs, metas, zb, zp, rin, rout, stage, rows, ysend, yrecv,
     ex, cm, sm, st, erow, upper, perm_g, perm_s, acc, xb, gacc, uacc, hb, yb,
     wgv, wuv, wdv,
     w_sem, m_send, m_recv, z_send, z_recv, p_send, p_recv, y_send, y_recv, r_send, r_recv,
 ):
     NZ, NX, T, D, FE, CAP = dm.NZ, dm.NX, dm.T, dm.D, dm.FE, dm.CAP
-    DQ, H, PL, RB, NR, HB, SR, KP, caps = dm.DQ, dm.H, dm.PL, dm.RB, dm.NR, dm.HB, dm.SR, dm.KP, dm.caps
+    DQ, H, PL, RB, NR, SR, KP, caps = dm.DQ, dm.H, dm.PL, dm.RB, dm.NR, dm.SR, dm.KP, dm.caps
     ep, x = lax.axis_index("ep"), lax.axis_index("tp")
     z, c = ep // 2, ep % 2
 
     def at_z(other):
         return {"ep": other * 2 + c, "tp": x}
+
+    def onward(direction):
+        return at_z((z + 1 - 2 * direction + NZ) % NZ)
+
+    def backward(direction):
+        return at_z((z - 1 + 2 * direction + NZ) % NZ)
 
     def in_plane(j):
         dc, dx = j // NX, j % NX
@@ -64,8 +69,8 @@
         return (j // NX) * NX + (NX - j % NX) % NX
 
     barrier = pltpu.get_barrier_semaphore()
-    for d in range(1, NZ):
-        pl.semaphore_signal(barrier, inc=1, device_id=at_z((z + d) % NZ), device_id_type=MESH)
+    for direction in range(2):
+        pl.semaphore_signal(barrier, inc=1, device_id=onward(direction), device_id_type=MESH)
     for j in range(1, PL):
         pl.semaphore_signal(barrier, inc=1, device_id=in_plane(j), device_id_type=MESH)
 
@@ -90,7 +95,9 @@
 
     lax.fori_loop(0, T // NB, norm_rows, 0)
 
-    metas[0] = meta[...]
+    for direction in range(2):
+        metas[direction, 0, 0:2, :] = ids_in[...].astype(F32)
+        metas[direction, 0, 2:4, :] = wts_in[...]
     r_id = lax.broadcasted_iota(I32, (NR, T), 0)
     j_id = r_id // RB
     dx_id, dc_id = j_id % NX, j_id // NX
@@ -107,36 +114,52 @@
     q_of, m_of = n_id // SR, n_id % SR
     perm_s[...] = jnp.where(a_id == (m_of // CAP) * RB + q_of * CAP + m_of % CAP, 1.0, 0.0).astype(BF)
 
-    pl.semaphore_wait(barrier, NZ - 1 + PL - 1)
-
-    meta_copies = [
-        pltpu.make_async_remote_copy(
-            src_ref=meta, dst_ref=metas.at[d], send_sem=m_send.at[d], recv_sem=m_recv.at[d],
-            device_id=at_z((z + d) % NZ), device_id_type=MESH,
-        )
-        for d in range(1, NZ)
-    ]
-    for copy in meta_copies:
-        copy.start()
-
     def z_copy(src, direction, k, q, rows_sent):
         return pltpu.make_async_remote_copy(
             src_ref=src, dst_ref=zb.at[direction, k - 1, q, pl.ds(0, rows_sent)],
             send_sem=z_send.at[direction, k - 1, q], recv_sem=z_recv.at[direction, k - 1, q],
-            device_id=at_z((z + 1 - 2 * direction + NZ) % NZ), device_id_type=MESH,
+            device_id=onward(direction), device_id_type=MESH,
         )
 
-    def send_own(i, _):
-        q, direction = i // 2, i % 2
-        z_copy(xs.at[q], direction, 1, q, caps[1]).start()
-        return 0
-
-    lax.fori_loop(0, 2 * Q, send_own, 0)
+    def m_copy(direction, k):
+        return pltpu.make_async_remote_copy(
+            src_ref=metas.at[direction, k - 1], dst_ref=metas.at[direction, k],
+            send_sem=m_send.at[direction, k], recv_sem=m_recv.at[direction, k],
+            device_id=onward(direction), device_id_type=MESH,
+        )
+
+    def relay_meta(direction, k):
+        m_copy(direction, k).wait_recv()
+
+        @pl.when(k < H)
+        def _():
+            m_copy(direction, k + 1).start()
+
+    def plane_copy(src, dst, t, j, send, recv):
+        if t < H:
+            here, there = src.at[t - 1, j], dst.at[t - 1, mirror(j)]
+        else:
+            here, there = src.at[H - 1, j, t - H], dst.at[H - 1, mirror(j), t - H]
+        return pltpu.make_async_remote_copy(
+            src_ref=here, dst_ref=there, send_sem=send.at[t - 1, j], recv_sem=recv.at[t - 1, mirror(j)],
+            device_id=in_plane(j), device_id_type=MESH,
+        )
+
+    def plane_start(src, dst, t, send, recv):
+        for j in range(1, PL):
+            plane_copy(src, dst, t, j, send, recv).start()
+
+    def plane_wait(src, dst, t, send, recv):
+        for j in range(1, PL):
+            plane_copy(src, dst, t, mirror(j), send, recv).wait_recv()
+
+    def plane_sent(src, dst, t, send, recv):
+        for j in range(1, PL):
+            plane_copy(src, dst, t, j, send, recv).wait_send()
 
     def build(direction, k):
-        d = k + direction * (NZ - 2 * k)
-        s = (z - d + NZ) % NZ
-        m = metas[d]
+        s = (z + NZ - k + 2 * k * direction) % NZ
+        m = metas[direction, k]
         ids = [m[i:i + 1, :].astype(I32) for i in range(2)]
         wts = [m[2 + i:3 + i, :] for i in range(2)]
         e = erow[...]
@@ -190,18 +213,65 @@
     def only_q_cols(v, q):
         return jnp.where(q_col == q, v.astype(F32), 0.0).astype(BF)
 
-    build(0, 0)
-    own = jnp.zeros((NR, DQ), F32)
-    for q in range(Q):
-        own = own + mm(only_q_rows(ex[0, 0], q), xs[q])
-    own = own.astype(BF).reshape(PL, RB, DQ)
-    stage[H - 1, :, 1] = own
-    rows[H - 1, 0, 1] = own[0]
-
-    for copy in meta_copies:
-        copy.wait()
-
-    def dispatch(k):
+    def own_block():
+        build(0, 0)
+        acc[0] = jnp.zeros((NR, DQ), F32)
+
+        def one(q, _):
+            acc[0] = acc[0] + mm(only_q_rows(ex[0, 0], q), xs[q])
+            return 0
+
+        lax.fori_loop(0, Q, one, 0)
+        own = acc[0].astype(BF).reshape(PL, RB, DQ)
+        stage[H - 1, :, 1] = own
+        rows[H - 1, 0, 1] = own[0]
+        plane_start(stage, rows, H + 1, p_send, p_recv)
+
+    def gather(k0):
+        for i in range(2):
+            k = k0 + i
+            plane_wait(stage, rows, k, p_send, p_recv)
+            if k == H:
+                plane_wait(stage, rows, H + 1, p_send, p_recv)
+            got = mm(perm_g[...], rows[k - 1].reshape(PR, DQ)).astype(BF).reshape(Q, SR, DQ)
+            xb[:, pl.ds(i * SR, SR), :] = got
+        gacc[...] = jnp.zeros_like(gacc)
+        uacc[...] = jnp.zeros_like(uacc)
+
+    def piece(i):
+        @pl.when(i < Q)
+        def _():
+            gacc[...] += mm(xb[i], wgv[i])
+            uacc[...] += mm(xb[i], wuv[i])
+
+        @pl.when(i == Q)
+        def _():
+            g = gacc[...]
+            hb[...] = ((g / (1.0 + jnp.exp(-g))) * uacc[...]).astype(BF)
+
+        @pl.when(i >= Q)
+        def _():
+            yb[i - Q] = mm(hb[...], wdv[i - Q]).astype(BF)
+
+    def scatter(k0):
+        for i in range(2):
+            k = k0 + i
+            v = yb[:, pl.ds(i * SR, SR), :].reshape(PR, DQ)
+            v = mm(perm_s[...], v).astype(BF).reshape(PL, 2, RB, DQ)
+            ysend[k - 1] = v
+            yrecv[k - 1, 0] = v[0]
+
+    def experts(k0):
+        gather(k0)
+
+        def one(i, _):
+            piece(i)
+            return 0
+
+        lax.fori_loop(0, 2 * Q, one, 0)
+        scatter(k0)
+
+    def dispatch(k, beside):
         ck = caps[k]
         acc[...] = jnp.zeros_like(acc)
 
@@ -213,18 +283,22 @@
                 cn = caps[k + 1]
                 if k + 1 >= KP:
                     p = k + 1 - KP
-                    zp[direction, p, q, pl.ds(0, cn), :] = mm(
-                        sm[direction, k, pl.ds(0, cn), pl.ds(0, ck)] if ck == T else sm[direction, k][:cn, :ck], data
-                    ).astype(BF)
+                    zp[direction, p, q, pl.ds(0, cn), :] = mm(sm[direction, k][:cn, :ck], data).astype(BF)
                     source = zp.at[direction, p, q, pl.ds(0, cn)]
                 else:
                     source = zb.at[direction, k - 1, q, pl.ds(0, cn)]
                 z_copy(source, direction, k + 1, q, cn).start()
+            if k == 1:
+                @pl.when(q + Q <= H)
+                def _():
+                    relay_meta(direction, q + Q)
             e = only_q_rows(ex[direction, k], q)
             if ck < T:
                 e = e[:, :ck]
             block = direction if k < H else 0
             acc[block] = acc[block] + mm(e, data)
+            if beside:
+                piece(i)
             return 0
 
         lax.fori_loop(0, 2 * Q, chunk, 0)
@@ -232,75 +306,58 @@
             v = acc[block].astype(BF).reshape(PL, RB, DQ)
             stage[k - 1, :, block] = v
             rows[k - 1, 0, block] = v[0]
-        for j in range(1, PL):
-            plane_copy(stage, rows, k, j, p_send, p_recv).start()
-
-    def plane_copy(src, dst, k, j, send, recv):
-        return pltpu.make_async_remote_copy(
-            src_ref=src.at[k - 1, j], dst_ref=dst.at[k - 1, mirror(j)],
-            send_sem=send.at[k - 1, j], recv_sem=recv.at[k - 1, mirror(j)],
-            device_id=in_plane(j), device_id_type=MESH,
-        )
-
-    def plane_wait(src, dst, k, send, recv):
-        for j in range(1, PL):
-            plane_copy(src, dst, k, mirror(j), send, recv).wait_recv()
-
-    def experts(k0):
-        BR = HB * SR
-        for i in range(HB):
-            k = k0 + i
-            plane_wait(stage, rows, k, p_send, p_recv)
-            got = mm(perm_g[...], rows[k - 1].reshape(PR, DQ)).astype(BF).reshape(Q, SR, DQ)
-            xb[:, pl.ds(i * SR, SR), :] = got
-        gacc[...] = jnp.zeros_like(gacc)
-        uacc[...] = jnp.zeros_like(uacc)
-
-        def inner(q, _):
-            v = xb[q]
-            gacc[...] += mm(v, wgv[q])
-            uacc[...] += mm(v, wuv[q])
-            return 0
-
-        lax.fori_loop(0, Q, inner, 0)
-        g = gacc[...]
-        hb[...] = ((g / (1.0 + jnp.exp(-g))) * uacc[...]).astype(BF)
-
-        def outer(q, _):
-            yb[q] = mm(hb[...], wdv[q]).astype(BF)
-            return 0
-
-        lax.fori_loop(0, Q, outer, 0)
-        for i in range(HB):
-            k = k0 + i
-            v = yb[:, pl.ds(i * SR, SR), :].reshape(PR, DQ)
-            v = mm(perm_s[...], v).astype(BF).reshape(PL, 2, RB, DQ)
-            ysend[k - 1] = v
-            yrecv[k - 1, 0] = v[0]
-            for j in range(1, PL):
-                plane_copy(ysend, yrecv, k, j, y_send, y_recv).start()
-
-    build_steps(1, min(3, H + 1))
-    built = min(3, H + 1)
+        plane_start(stage, rows, k, p_send, p_recv)
+
+    firsts = list(range(1, H, 2))
+    beside = {k0 + 3: k0 for k0 in firsts if k0 + 3 <= H - 2}
+    after = [k0 for k0 in firsts if k0 + 3 > H - 2]
+
+    pl.semaphore_wait(barrier, 2 + PL - 1)
+    for direction in range(2):
+        m_copy(direction, 1).start()
+    for q in range(Q):
+        for direction in range(2):
+            z_copy(xs.at[q], direction, 1, q, caps[1]).start()
+        if q == 0:
+            own_block()
+        if 1 <= q + 1 < Q and q + 1 <= H:
+            for direction in range(2):
+                relay_meta(direction, q + 1)
+        if q == 0:
+            build_steps(1, 2)
+
+    dispatch(1, False)
+    for k in range(2 * Q, H + 1):
+        for direction in range(2):
+            relay_meta(direction, k)
+    for copy in weight_copies:
+        copy.wait()
+    built = 2
     for k in range(1, H + 1):
-        dispatch(k)
-        if built <= H:
-            nxt = min(built + 2, H + 1)
+        if k > 1:
+            if k in beside:
+                gather(beside[k])
+            dispatch(k, k in beside)
+            if k in beside:
+                scatter(beside[k])
+                for i in range(2):
+                    plane_start(ysend, yrecv, beside[k] + i, y_send, y_recv)
+        nxt = min(built + 2, H + 1)
+        if built < nxt:
             build_steps(built, nxt)
-            built = nxt
-        if k == 1:
-            for copy in weight_copies:
-                copy.wait()
-        if k == HB + 1:
-            experts(1)
-    experts(HB + 1)
+        built = nxt
+    for k0 in after:
+        experts(k0)
+    for k in range(H, after[0] - 1, -1):
+        plane_start(ysend, yrecv, k, y_send, y_recv)
+    plane_start(ysend, yrecv, H + 1, y_send, y_recv)
 
     def r_copy(direction, k, q):
         return pltpu.make_async_remote_copy(
             src_ref=rout.at[direction, k - 1, q, pl.ds(0, caps[k])],
             dst_ref=rin.at[direction, k - 1, q, pl.ds(0, caps[k])],
             send_sem=r_send.at[direction, k - 1, q], recv_sem=r_recv.at[direction, k - 1, q],
-            device_id=at_z((z - 1 + 2 * direction + NZ) % NZ), device_id_type=MESH,
+            device_id=backward(direction), device_id_type=MESH,
         )
 
     for k in range(H, 0, -1):
@@ -322,10 +379,20 @@
                     v = v + far.astype(F32)
             rout[direction, k - 1, q, pl.ds(0, ck), :] = v.astype(BF)
             r_copy(direction, k, q).start()
+            z_copy(xs.at[q, pl.ds(0, ck)], direction, k, q, ck).wait_send()
+            if k < H:
+                r_copy(direction, k + 1, q).wait_send()
             return 0
 
         lax.fori_loop(0, 2 * Q, back, 0)
-
+        plane_sent(stage, rows, k, p_send, p_recv)
+        plane_sent(ysend, yrecv, k, y_send, y_recv)
+        for direction in range(2):
+            m_copy(direction, k).wait_send()
+
+    plane_sent(stage, rows, H + 1, p_send, p_recv)
+    plane_sent(ysend, yrecv, H + 1, y_send, y_recv)
+    plane_wait(ysend, yrecv, H + 1, y_send, y_recv)
     y_own = yrecv[H - 1, :, 1].reshape(NR, DQ)
     for q in range(Q):
         v = mm(only_q_cols(cm[0, 0], q), y_own)
@@ -333,18 +400,9 @@
             r_copy(direction, 1, q).wait_recv()
             v = v + rin[direction, 0, q].astype(F32)
         out[:, q * DQ:(q + 1) * DQ] = v.astype(BF)
-
-    for k in range(1, H + 1):
-        def drained(i, _, k=k):
-            q, direction = i // 2, i % 2
-            z_copy(xs.at[q, pl.ds(0, caps[k])], direction, k, q, caps[k]).wait_send()
-            r_copy(direction, k, q).wait_send()
-            return 0
-
-        lax.fori_loop(0, 2 * Q, drained, 0)
-        for j in range(1, PL):
-            plane_copy(stage, rows, k, j, p_send, p_recv).wait_send()
-            plane_copy(ysend, yrecv, k, j, y_send, y_recv).wait_send()
+    for q in range(Q):
+        for direction in range(2):
+            r_copy(direction, 1, q).wait_send()
 
 
 def body(hidden_in, expert_ids, route_weights, norm_gain, gate_proj, up_proj, down_proj):
@@ -354,21 +412,18 @@
     fe = gate_proj.shape[2]
     cap = max(2, 2 * chosen * tokens // (ep * tp))
     dm = Dims(ep, tp, tokens, width, fe, cap)
-    meta = jnp.concatenate(
-        [expert_ids.T.astype(F32), route_weights.T, jnp.zeros((4, tokens), F32)], axis=0
-    )
-    H, T, DQ, PL, RB, NR, NZ, SR, HB = dm.H, dm.T, dm.DQ, dm.PL, dm.RB, dm.NR, dm.NZ, dm.SR, dm.HB
+    H, T, DQ, PL, RB, NR, SR = dm.H, dm.T, dm.DQ, dm.PL, dm.RB, dm.NR, dm.SR
     vm = pltpu.VMEM
     packed = max(1, H - dm.KP + 1)
     dma = pltpu.SemaphoreType.DMA
     return pl.pallas_call(
         functools.partial(kernel, dm),
         out_shape=jax.ShapeDtypeStruct((tokens, width), BF),
-        in_specs=[pl.BlockSpec(memory_space=vm)] * 3 + [pl.BlockSpec(memory_space=pl.ANY)] * 3,
+        in_specs=[pl.BlockSpec(memory_space=vm)] * 4 + [pl.BlockSpec(memory_space=pl.ANY)] * 3,
         out_specs=pl.BlockSpec(memory_space=vm),
         scratch_shapes=[
             vm((Q, T, DQ), BF),
-            vm((NZ, 8, T), F32),
+            vm((2, H + 1, 4, T), F32),
             vm((2, H, Q, T, DQ), BF),
             vm((2, packed, Q, dm.caps[min(dm.KP, H)], DQ), BF),
             vm((2, H, Q, T, DQ), BF),
@@ -386,23 +441,23 @@
             vm((Q * SR, Q * SR), BF),
             vm((Q * SR, Q * SR), BF),
             vm((2, NR, DQ), F32),
-            vm((Q, HB * SR, DQ), BF),
-            vm((HB * SR, fe), F32),
-            vm((HB * SR, fe), F32),
-            vm((HB * SR, fe), BF),
-            vm((Q, HB * SR, DQ), BF),
+            vm((Q, 2 * SR, DQ), BF),
+            vm((2 * SR, fe), F32),
+            vm((2 * SR, fe), F32),
+            vm((2 * SR, fe), BF),
+            vm((Q, 2 * SR, DQ), BF),
             vm((Q, DQ, fe), BF),
             vm((Q, DQ, fe), BF),
             vm((Q, fe, DQ), BF),
             dma((3, Q)),
-            dma((NZ,)),
-            dma((NZ,)),
+            dma((2, H + 1)),
+            dma((2, H + 1)),
             dma((2, H, Q)),
             dma((2, H, Q)),
-            dma((H, PL)),
-            dma((H, PL)),
-            dma((H, PL)),
-            dma((H, PL)),
+            dma((H + 1, PL)),
+            dma((H + 1, PL)),
+            dma((H + 1, PL)),
+            dma((H + 1, PL)),
             dma((2, H, Q)),
             dma((2, H, Q)),
         ],
@@ -410,7 +465,7 @@
             collective_id=0, has_side_effects=True, vmem_limit_bytes=66 * 1000 * 1000
         ),
         name="routed_experts",
-    )(hidden_in, meta, norm_gain.reshape(1, width), gate_proj, up_proj, down_proj)
+    )(hidden_in, expert_ids.T, route_weights.T, norm_gain.reshape(1, width), gate_proj, up_proj, down_proj)
 
 
 def solution(mesh):

time: 212 us -> 196 us (0.925)
  Pallas kernels: 207 us -> 194 us
    pallas_call x1, Pallas kernels: 207 us -> 194 us  [body(): pl.pallas_call(functools.partial(kernel, dm), out_shape=jax.ShapeDtypeStr...]
where the time goes in v2:
time: 196 us
  Pallas kernels  194 us (99%)
    pallas_call x1, Pallas kernels, body(): pl.pallas_call(functools.partial(kernel, dm), out_shape=jax.ShapeDtypeStr...  194 us

profile of v2, /device:TPU:33, one launch (start us, length us, event | category | flops | bytes accessed | tf_op | source)
XLA Modules:
  0.0 196.3 jit_solution(10559881471805045092)
XLA Ops:
  0.0 194.4 %routed_experts.1 = bf16[128,2048]{1,0:T(8,128)(2,1)} custom-call(bf16[128,2048]{1,0:T(8,128)(2,1)} %hid.1, s32[2,128]{1,0:T(2,128)} %bitcast.4, f32[2,128]{1,0:T(2,128)} %bitcast.5, f32[1,2048]{1,0:T(1,128)} %bitcast.3, bf16[1,2048,512]{2,1,0:T(8,128)(2,1)} %wg.1, bf16[1,2048,512]{2,1,0:T(8,128)(2,1)} %wu.1, bf16[1,512,2048]{2,1,0:T(8,128)(2,1)} %wd.1), custom_call_target="tpu_custom_call" | custom-call | tf_op jit(solution)/shard_map/routed_experts/pallas_call | solution.py:419
  194.4 1.9 copy.9

commit v3 on v2

--- a/solution.py
+++ b/solution.py
@@ -277,6 +277,11 @@
 
         def chunk(i, _):
             q, direction = i // 2, i % 2
+            base = Q - 1 + 2 * (k - 1)
+            if base <= H:
+                @pl.when((q % 2 == 1) & (base + q // 2 <= H))
+                def _():
+                    relay_meta(direction, base + q // 2)
             z_copy(zb.at[direction, k - 1, q, pl.ds(0, ck)], direction, k, q, ck).wait_recv()
             data = zb[direction, k - 1, q, pl.ds(0, ck), :]
             if k < H:
@@ -288,10 +293,6 @@
                 else:
                     source = zb.at[direction, k - 1, q, pl.ds(0, cn)]
                 z_copy(source, direction, k + 1, q, cn).start()
-            if k == 1:
-                @pl.when(q + Q <= H)
-                def _():
-                    relay_meta(direction, q + Q)
             e = only_q_rows(ex[direction, k], q)
             if ck < T:
                 e = e[:, :ck]
@@ -315,21 +316,19 @@
     pl.semaphore_wait(barrier, 2 + PL - 1)
     for direction in range(2):
         m_copy(direction, 1).start()
-    for q in range(Q):
+    for q in range(2):
         for direction in range(2):
             z_copy(xs.at[q], direction, 1, q, caps[1]).start()
-        if q == 0:
-            own_block()
-        if 1 <= q + 1 < Q and q + 1 <= H:
-            for direction in range(2):
-                relay_meta(direction, q + 1)
-        if q == 0:
+    own_block()
+    for q in range(2, Q):
+        for direction in range(2):
+            relay_meta(direction, q - 1)
+        for direction in range(2):
+            z_copy(xs.at[q], direction, 1, q, caps[1]).start()
+        if q == 2:
             build_steps(1, 2)
 
     dispatch(1, False)
-    for k in range(2 * Q, H + 1):
-        for direction in range(2):
-            relay_meta(direction, k)
     for copy in weight_copies:
         copy.wait()
     built = 2

time: 196 us -> 193 us (0.985)
  Pallas kernels: 194 us -> 191 us
    pallas_call x1, Pallas kernels: 194 us -> 191 us  [body(): pl.pallas_call(functools.partial(kernel, dm), out_shape=jax.ShapeDtypeStr...]
where the time goes in v3:
time: 193 us
  Pallas kernels  191 us (99%)
    pallas_call x1, Pallas kernels, body(): pl.pallas_call(functools.partial(kernel, dm), out_shape=jax.ShapeDtypeStr...  191 us

profile of v3, /device:TPU:33, one launch (start us, length us, event | category | flops | bytes accessed | tf_op | source)
XLA Modules:
  0.0 193.1 jit_solution(14408615551500483197)
XLA Ops:
  0.0 191.2 %routed_experts.1 = bf16[128,2048]{1,0:T(8,128)(2,1)} custom-call(bf16[128,2048]{1,0:T(8,128)(2,1)} %hid.1, s32[2,128]{1,0:T(2,128)} %bitcast.4, f32[2,128]{1,0:T(2,128)} %bitcast.5, f32[1,2048]{1,0:T(1,128)} %bitcast.3, bf16[1,2048,512]{2,1,0:T(8,128)(2,1)} %wg.1, bf16[1,2048,512]{2,1,0:T(8,128)(2,1)} %wu.1, bf16[1,512,2048]{2,1,0:T(8,128)(2,1)} %wd.1), custom_call_target="tpu_custom_call" | custom-call | tf_op jit(solution)/shard_map/routed_experts/pallas_call | solution.py:418
  191.2 1.9 copy.9

commit v4 on v3

--- a/solution.py
+++ b/solution.py
@@ -41,11 +41,12 @@
 
 
 def kernel(
-    dm, hid, ids_in, wts_in, gain, wg, wu, wd, out,
+    dm, hid_in, ids_in, wts_in, gain_in, wg, wu, wd, out_ref,
+    hid, idv, wtv, gain, out,
     xs, metas, zb, zp, rin, rout, stage, rows, ysend, yrecv,
     ex, cm, sm, st, erow, upper, perm_g, perm_s, acc, xb, gacc, uacc, hb, yb,
     wgv, wuv, wdv,
-    w_sem, m_send, m_recv, z_send, z_recv, p_send, p_recv, y_send, y_recv, r_send, r_recv,
+    i_sem, o_sem, w_sem, m_send, m_recv, z_send, z_recv, p_send, p_recv, y_send, y_recv, r_send, r_recv,
 ):
     NZ, NX, T, D, FE, CAP = dm.NZ, dm.NX, dm.T, dm.D, dm.FE, dm.CAP
     DQ, H, PL, RB, NR, SR, KP, caps = dm.DQ, dm.H, dm.PL, dm.RB, dm.NR, dm.SR, dm.KP, dm.caps
@@ -74,6 +75,18 @@
     for j in range(1, PL):
         pl.semaphore_signal(barrier, inc=1, device_id=in_plane(j), device_id_type=MESH)
 
+    small_copies = [
+        pltpu.make_async_copy(ids_in, idv, i_sem.at[0]),
+        pltpu.make_async_copy(wts_in, wtv, i_sem.at[1]),
+        pltpu.make_async_copy(gain_in, gain, i_sem.at[2]),
+    ]
+    part = T // 4
+    hid_copies = [
+        pltpu.make_async_copy(hid_in.at[pl.ds(i * part, part)], hid.at[pl.ds(i * part, part)], i_sem.at[3 + i])
+        for i in range(4)
+    ]
+    for copy in [small_copies[2]] + hid_copies + small_copies[:2]:
+        copy.start()
     weight_copies = []
     for q in range(Q):
         weight_copies.append(pltpu.make_async_copy(wg.at[0, pl.ds(q * DQ, DQ)], wgv.at[q], w_sem.at[0, q]))
@@ -82,22 +95,6 @@
     for copy in weight_copies:
         copy.start()
 
-    NB = 16
-
-    def norm_rows(b, _):
-        r = pl.ds(pl.multiple_of(b * NB, NB), NB)
-        v = hid[r, :].astype(F32)
-        scale = lax.rsqrt(jnp.mean(v * v, axis=-1, keepdims=True) + 1e-06)
-        n = ((v * scale) * gain[...]).astype(BF)
-        for q in range(Q):
-            xs[q, r, :] = n[:, q * DQ:(q + 1) * DQ]
-        return 0
-
-    lax.fori_loop(0, T // NB, norm_rows, 0)
-
-    for direction in range(2):
-        metas[direction, 0, 0:2, :] = ids_in[...].astype(F32)
-        metas[direction, 0, 2:4, :] = wts_in[...]
     r_id = lax.broadcasted_iota(I32, (NR, T), 0)
     j_id = r_id // RB
     dx_id, dc_id = j_id % NX, j_id // NX
@@ -114,6 +111,28 @@
     q_of, m_of = n_id // SR, n_id % SR
     perm_s[...] = jnp.where(a_id == (m_of // CAP) * RB + q_of * CAP + m_of % CAP, 1.0, 0.0).astype(BF)
 
+    small_copies[2].wait()
+    NB = min(16, part)
+
+    def norm_rows(b, _):
+        r = pl.ds(pl.multiple_of(b * NB, NB), NB)
+        v = hid[r, :].astype(F32)
+        scale = lax.rsqrt(jnp.mean(v * v, axis=-1, keepdims=True) + 1e-06)
+        n = ((v * scale) * gain[...]).astype(BF)
+        for q in range(Q):
+            xs[q, r, :] = n[:, q * DQ:(q + 1) * DQ]
+        return 0
+
+    for i in range(4):
+        hid_copies[i].wait()
+        lax.fori_loop(i * (part // NB), (i + 1) * (part // NB), norm_rows, 0)
+
+    small_copies[0].wait()
+    small_copies[1].wait()
+    for direction in range(2):
+        metas[direction, 0, 0:2, :] = idv[...].astype(F32)
+        metas[direction, 0, 2:4, :] = wtv[...]
+
     def z_copy(src, direction, k, q, rows_sent):
         return pltpu.make_async_remote_copy(
             src_ref=src, dst_ref=zb.at[direction, k - 1, q, pl.ds(0, rows_sent)],
@@ -130,10 +149,11 @@
 
     def relay_meta(direction, k):
         m_copy(direction, k).wait_recv()
-
-        @pl.when(k < H)
-        def _():
+        if k < H:
             m_copy(direction, k + 1).start()
+
+    relay_at = {(2, 3): 3, (3, 1): 4, (3, 3): 5, (4, 1): 6, (4, 3): 7, (5, 1): 8}
+    assert H <= 8
 
     def plane_copy(src, dst, t, j, send, recv):
         if t < H:
@@ -277,11 +297,11 @@
 
         def chunk(i, _):
             q, direction = i // 2, i % 2
-            base = Q - 1 + 2 * (k - 1)
-            if base <= H:
-                @pl.when((q % 2 == 1) & (base + q // 2 <= H))
-                def _():
-                    relay_meta(direction, base + q // 2)
+            for at_q in range(Q):
+                if relay_at.get((k, at_q), H + 1) <= H:
+                    @pl.when(q == at_q)
+                    def _():
+                        relay_meta(direction, relay_at[k, at_q])
             z_copy(zb.at[direction, k - 1, q, pl.ds(0, ck)], direction, k, q, ck).wait_recv()
             data = zb[direction, k - 1, q, pl.ds(0, ck), :]
             if k < H:
@@ -312,43 +332,46 @@
     firsts = list(range(1, H, 2))
     beside = {k0 + 3: k0 for k0 in firsts if k0 + 3 <= H - 2}
     after = [k0 for k0 in firsts if k0 + 3 > H - 2]
+    sent = []
 
     pl.semaphore_wait(barrier, 2 + PL - 1)
     for direction in range(2):
         m_copy(direction, 1).start()
-    for q in range(2):
+    for q in range(Q):
         for direction in range(2):
             z_copy(xs.at[q], direction, 1, q, caps[1]).start()
     own_block()
-    for q in range(2, Q):
-        for direction in range(2):
-            relay_meta(direction, q - 1)
-        for direction in range(2):
-            z_copy(xs.at[q], direction, 1, q, caps[1]).start()
-        if q == 2:
-            build_steps(1, 2)
-
+    for direction in range(2):
+        relay_meta(direction, 1)
+    build_steps(1, 2)
     dispatch(1, False)
+    for direction in range(2):
+        if H > 1:
+            relay_meta(direction, 2)
+    build_steps(2, min(3, H + 1))
     for copy in weight_copies:
         copy.wait()
-    built = 2
-    for k in range(1, H + 1):
-        if k > 1:
-            if k in beside:
-                gather(beside[k])
-            dispatch(k, k in beside)
-            if k in beside:
-                scatter(beside[k])
+    builds_after = {2: (3, 4), 3: (4, 6), 4: (6, 8), 5: (8, 9)}
+    for k in range(2, H + 1):
+        if k in beside:
+            gather(beside[k])
+        dispatch(k, k in beside)
+        if k in beside:
+            scatter(beside[k])
+            if k < KP:
+                sent.append(beside[k])
                 for i in range(2):
                     plane_start(ysend, yrecv, beside[k] + i, y_send, y_recv)
-        nxt = min(built + 2, H + 1)
-        if built < nxt:
-            build_steps(built, nxt)
-        built = nxt
+        lo, hi = builds_after.get(k, (H + 1, H + 1))
+        if lo <= H:
+            build_steps(lo, min(hi, H + 1))
     for k0 in after:
         experts(k0)
     for k in range(H, after[0] - 1, -1):
         plane_start(ysend, yrecv, k, y_send, y_recv)
+    for k0 in reversed([k0 for k0 in beside.values() if k0 not in sent]):
+        for i in (1, 0):
+            plane_start(ysend, yrecv, k0 + i, y_send, y_recv)
     plane_start(ysend, yrecv, H + 1, y_send, y_recv)
 
     def r_copy(direction, k, q):
@@ -392,16 +415,22 @@
     plane_sent(stage, rows, H + 1, p_send, p_recv)
     plane_sent(ysend, yrecv, H + 1, y_send, y_recv)
     plane_wait(ysend, yrecv, H + 1, y_send, y_recv)
+
+    def out_copy(q):
+        return pltpu.make_async_copy(out.at[q], out_ref.at[:, pl.ds(q * DQ, DQ)], o_sem.at[q])
+
     y_own = yrecv[H - 1, :, 1].reshape(NR, DQ)
     for q in range(Q):
         v = mm(only_q_cols(cm[0, 0], q), y_own)
         for direction in range(2):
             r_copy(direction, 1, q).wait_recv()
             v = v + rin[direction, 0, q].astype(F32)
-        out[:, q * DQ:(q + 1) * DQ] = v.astype(BF)
+        out[q] = v.astype(BF)
+        out_copy(q).start()
     for q in range(Q):
         for direction in range(2):
             r_copy(direction, 1, q).wait_send()
+        out_copy(q).wait()
 
 
 def body(hidden_in, expert_ids, route_weights, norm_gain, gate_proj, up_proj, down_proj):
@@ -418,9 +447,14 @@
     return pl.pallas_call(
         functools.partial(kernel, dm),
         out_shape=jax.ShapeDtypeStruct((tokens, width), BF),
-        in_specs=[pl.BlockSpec(memory_space=vm)] * 4 + [pl.BlockSpec(memory_space=pl.ANY)] * 3,
-        out_specs=pl.BlockSpec(memory_space=vm),
+        in_specs=[pl.BlockSpec(memory_space=pl.ANY)] * 7,
+        out_specs=pl.BlockSpec(memory_space=pl.ANY),
         scratch_shapes=[
+            vm((tokens, width), BF),
+            vm((2, tokens), I32),
+            vm((2, tokens), F32),
+            vm((1, width), F32),
+            vm((Q, T, DQ), BF),
             vm((Q, T, DQ), BF),
             vm((2, H + 1, 4, T), F32),
             vm((2, H, Q, T, DQ), BF),
@@ -448,6 +482,8 @@
             vm((Q, DQ, fe), BF),
             vm((Q, DQ, fe), BF),
             vm((Q, fe, DQ), BF),
+            dma((7,)),
+            dma((Q,)),
             dma((3, Q)),
             dma((2, H + 1)),
             dma((2, H + 1)),

time: 193 us -> 190 us (0.984)
  Pallas kernels: 191 us -> 188 us
    pallas_call x1, Pallas kernels: 191 us -> 188 us  [body(): pl.pallas_call(functools.partial(kernel, dm), out_shape=jax.ShapeDtypeStr...]
where the time goes in v4:
time: 190 us
  Pallas kernels  188 us (99%)
    pallas_call x1, Pallas kernels, body(): pl.pallas_call(functools.partial(kernel, dm), out_shape=jax.ShapeDtypeStr...  188 us

profile of v4, /device:TPU:33, one launch (start us, length us, event | category | flops | bytes accessed | tf_op | source)
XLA Modules:
  0.0 189.8 jit_solution(2227673004650190553)
XLA Ops:
  0.0 187.9 %routed_experts.1 = bf16[128,2048]{1,0:T(8,128)(2,1)} custom-call(bf16[128,2048]{1,0:T(8,128)(2,1)} %hid_in.1, s32[2,128]{1,0:T(2,128)} %bitcast.4, f32[2,128]{1,0:T(2,128)} %bitcast.5, f32[1,2048]{1,0:T(1,128)} %bitcast.3, bf16[1,2048,512]{2,1,0:T(8,128)(2,1)} %wg.1, bf16[1,2048,512]{2,1,0:T(8,128)(2,1)} %wu.1, bf16[1,512,2048]{2,1,0:T(8,128)(2,1)} %wd.1), custom_call_target="tpu_custom_call" | custom-call | tf_op jit(solution)/shard_map/routed_experts/pallas_call | solution.py:447
  188.0 1.9 copy.9

commit v5 on v4

--- a/solution.py
+++ b/solution.py
@@ -92,9 +92,6 @@
         weight_copies.append(pltpu.make_async_copy(wg.at[0, pl.ds(q * DQ, DQ)], wgv.at[q], w_sem.at[0, q]))
         weight_copies.append(pltpu.make_async_copy(wu.at[0, pl.ds(q * DQ, DQ)], wuv.at[q], w_sem.at[1, q]))
         weight_copies.append(pltpu.make_async_copy(wd.at[0, :, pl.ds(q * DQ, DQ)], wdv.at[q], w_sem.at[2, q]))
-    for copy in weight_copies:
-        copy.start()
-
     r_id = lax.broadcasted_iota(I32, (NR, T), 0)
     j_id = r_id // RB
     dx_id, dc_id = j_id % NX, j_id // NX
@@ -152,7 +149,7 @@
         if k < H:
             m_copy(direction, k + 1).start()
 
-    relay_at = {(2, 3): 3, (3, 1): 4, (3, 3): 5, (4, 1): 6, (4, 3): 7, (5, 1): 8}
+    relay_at = {(1, 3): 2, (2, 2): 3, (3, 1): 4, (4, 0): 5, (4, 3): 6, (5, 2): 7, (6, 1): 8}
     assert H <= 8
 
     def plane_copy(src, dst, t, j, send, recv):
@@ -340,18 +337,17 @@
     for q in range(Q):
         for direction in range(2):
             z_copy(xs.at[q], direction, 1, q, caps[1]).start()
+    for copy in weight_copies:
+        copy.start()
     own_block()
     for direction in range(2):
         relay_meta(direction, 1)
     build_steps(1, 2)
     dispatch(1, False)
-    for direction in range(2):
-        if H > 1:
-            relay_meta(direction, 2)
     build_steps(2, min(3, H + 1))
     for copy in weight_copies:
         copy.wait()
-    builds_after = {2: (3, 4), 3: (4, 6), 4: (6, 8), 5: (8, 9)}
+    builds_after = {2: (3, 4), 3: (4, 5), 4: (5, 7), 5: (7, 8), 6: (8, 9)}
     for k in range(2, H + 1):
         if k in beside:
             gather(beside[k])

time: 190 us -> 189 us (level)
  no operation moved by 1% of the time
where the time goes in v5:
time: 189 us
  Pallas kernels  187 us (99%)
    pallas_call x1, Pallas kernels, body(): pl.pallas_call(functools.partial(kernel, dm), out_shape=jax.ShapeDtypeStr...  187 us

profile of v5, /device:TPU:33, one launch (start us, length us, event | category | flops | bytes accessed | tf_op | source)
XLA Modules:
  0.0 189.1 jit_solution(11165055241874519068)
XLA Ops:
  0.0 187.2 %routed_experts.1 = bf16[128,2048]{1,0:T(8,128)(2,1)} custom-call(bf16[128,2048]{1,0:T(8,128)(2,1)} %hid_in.1, s32[2,128]{1,0:T(2,128)} %bitcast.4, f32[2,128]{1,0:T(2,128)} %bitcast.5, f32[1,2048]{1,0:T(1,128)} %bitcast.3, bf16[1,2048,512]{2,1,0:T(8,128)(2,1)} %wg.1, bf16[1,2048,512]{2,1,0:T(8,128)(2,1)} %wu.1, bf16[1,512,2048]{2,1,0:T(8,128)(2,1)} %wd.1), custom_call_target="tpu_custom_call" | custom-call | tf_op jit(solution)/shard_map/routed_experts/pallas_call | solution.py:443
  187.2 1.9 copy.9

commit v6 on v5

--- a/solution.py
+++ b/solution.py
@@ -133,14 +133,14 @@
     def z_copy(src, direction, k, q, rows_sent):
         return pltpu.make_async_remote_copy(
             src_ref=src, dst_ref=zb.at[direction, k - 1, q, pl.ds(0, rows_sent)],
-            send_sem=z_send.at[direction, k - 1, q], recv_sem=z_recv.at[direction, k - 1, q],
+            send_sem=z_send.at[k - 1], recv_sem=z_recv.at[direction, k - 1, q],
             device_id=onward(direction), device_id_type=MESH,
         )
 
     def m_copy(direction, k):
         return pltpu.make_async_remote_copy(
             src_ref=metas.at[direction, k - 1], dst_ref=metas.at[direction, k],
-            send_sem=m_send.at[direction, k], recv_sem=m_recv.at[direction, k],
+            send_sem=m_send.at[0], recv_sem=m_recv.at[direction, k],
             device_id=onward(direction), device_id_type=MESH,
         )
 
@@ -152,27 +152,31 @@
     relay_at = {(1, 3): 2, (2, 2): 3, (3, 1): 4, (4, 0): 5, (4, 3): 6, (5, 2): 7, (6, 1): 8}
     assert H <= 8
 
-    def plane_copy(src, dst, t, j, send, recv):
-        if t < H:
-            here, there = src.at[t - 1, j], dst.at[t - 1, mirror(j)]
-        else:
-            here, there = src.at[H - 1, j, t - H], dst.at[H - 1, mirror(j), t - H]
+    def blocks(ref, t, j):
+        return ref.at[t - 1, j] if t < H else ref.at[H - 1, j, t - H]
+
+    def plane_copy(src, dst, t, j, to, send, recv):
         return pltpu.make_async_remote_copy(
-            src_ref=here, dst_ref=there, send_sem=send.at[t - 1, j], recv_sem=recv.at[t - 1, mirror(j)],
-            device_id=in_plane(j), device_id_type=MESH,
+            src_ref=blocks(src, t, j), dst_ref=blocks(dst, t, to), send_sem=send.at[t - 1], recv_sem=recv.at[t - 1],
+            device_id=in_plane(1 if j is others else j), device_id_type=MESH,
         )
+
+    others = pl.ds(1, PL - 1)
 
     def plane_start(src, dst, t, send, recv):
         for j in range(1, PL):
-            plane_copy(src, dst, t, j, send, recv).start()
+            plane_copy(src, dst, t, j, mirror(j), send, recv).start()
 
     def plane_wait(src, dst, t, send, recv):
-        for j in range(1, PL):
-            plane_copy(src, dst, t, mirror(j), send, recv).wait_recv()
+        plane_copy(src, dst, t, others, others, send, recv).wait_recv()
 
     def plane_sent(src, dst, t, send, recv):
-        for j in range(1, PL):
-            plane_copy(src, dst, t, j, send, recv).wait_send()
+        plane_copy(src, dst, t, others, others, send, recv).wait_send()
+
+    def all_sent(src, send, recv):
+        pltpu.make_async_remote_copy(
+            src_ref=src, dst_ref=src, send_sem=send, recv_sem=recv, device_id=onward(0), device_id_type=MESH
+        ).wait_send()
 
     def build(direction, k):
         s = (z + NZ - k + 2 * k * direction) % NZ
@@ -270,15 +274,16 @@
         def _():
             yb[i - Q] = mm(hb[...], wdv[i - Q]).astype(BF)
 
-    def scatter(k0):
-        for i in range(2):
+    def scatter(k0, then=lambda k: None):
+        for i in (1, 0):
             k = k0 + i
             v = yb[:, pl.ds(i * SR, SR), :].reshape(PR, DQ)
             v = mm(perm_s[...], v).astype(BF).reshape(PL, 2, RB, DQ)
             ysend[k - 1] = v
             yrecv[k - 1, 0] = v[0]
-
-    def experts(k0):
+            then(k)
+
+    def experts(k0, then=lambda k: None):
         gather(k0)
 
         def one(i, _):
@@ -286,7 +291,7 @@
             return 0
 
         lax.fori_loop(0, 2 * Q, one, 0)
-        scatter(k0)
+        scatter(k0, then)
 
     def dispatch(k, beside):
         ck = caps[k]
@@ -331,6 +336,10 @@
     after = [k0 for k0 in firsts if k0 + 3 > H - 2]
     sent = []
 
+    def send_results(k):
+        plane_start(ysend, yrecv, k, y_send, y_recv)
+
+
     pl.semaphore_wait(barrier, 2 + PL - 1)
     for direction in range(2):
         m_copy(direction, 1).start()
@@ -347,34 +356,33 @@
     build_steps(2, min(3, H + 1))
     for copy in weight_copies:
         copy.wait()
-    builds_after = {2: (3, 4), 3: (4, 5), 4: (5, 7), 5: (7, 8), 6: (8, 9)}
+    builds_after = {2: (3, 4), 3: (4, 5), 4: (5, 7), 5: (7, 8), 7: (8, 9)}
     for k in range(2, H + 1):
         if k in beside:
             gather(beside[k])
         dispatch(k, k in beside)
-        if k in beside:
-            scatter(beside[k])
-            if k < KP:
-                sent.append(beside[k])
-                for i in range(2):
-                    plane_start(ysend, yrecv, beside[k] + i, y_send, y_recv)
+        if k in beside and k < KP:
+            scatter(beside[k], send_results)
+            sent.append(beside[k])
         lo, hi = builds_after.get(k, (H + 1, H + 1))
         if lo <= H:
             build_steps(lo, min(hi, H + 1))
-    for k0 in after:
+    late = [k0 for k0 in beside.values() if k0 not in sent]
+    for k0 in late:
+        scatter(k0)
+    for k0 in after[:-1]:
         experts(k0)
-    for k in range(H, after[0] - 1, -1):
-        plane_start(ysend, yrecv, k, y_send, y_recv)
-    for k0 in reversed([k0 for k0 in beside.values() if k0 not in sent]):
+    experts(after[-1], send_results)
+    for k0 in list(reversed(after[:-1])) + list(reversed(late)):
         for i in (1, 0):
-            plane_start(ysend, yrecv, k0 + i, y_send, y_recv)
-    plane_start(ysend, yrecv, H + 1, y_send, y_recv)
+            send_results(k0 + i)
+    send_results(H + 1)
 
     def r_copy(direction, k, q):
         return pltpu.make_async_remote_copy(
             src_ref=rout.at[direction, k - 1, q, pl.ds(0, caps[k])],
             dst_ref=rin.at[direction, k - 1, q, pl.ds(0, caps[k])],
-            send_sem=r_send.at[direction, k - 1, q], recv_sem=r_recv.at[direction, k - 1, q],
+            send_sem=r_send.at[k - 1], recv_sem=r_recv.at[direction, k - 1, q],
             device_id=backward(direction), device_id_type=MESH,
         )
 
@@ -397,17 +405,15 @@
                     v = v + far.astype(F32)
             rout[direction, k - 1, q, pl.ds(0, ck), :] = v.astype(BF)
             r_copy(direction, k, q).start()
-            z_copy(xs.at[q, pl.ds(0, ck)], direction, k, q, ck).wait_send()
-            if k < H:
-                r_copy(direction, k + 1, q).wait_send()
             return 0
 
         lax.fori_loop(0, 2 * Q, back, 0)
         plane_sent(stage, rows, k, p_send, p_recv)
         plane_sent(ysend, yrecv, k, y_send, y_recv)
-        for direction in range(2):
-            m_copy(direction, k).wait_send()
-
+        all_sent(zb.at[:, k - 1, :, pl.ds(0, ck)], z_send.at[k - 1], z_recv.at[0, k - 1, 0])
+        if k < H:
+            all_sent(rout.at[:, k, :, pl.ds(0, caps[k + 1])], r_send.at[k], r_recv.at[0, k, 0])
+    all_sent(metas.at[:, pl.ds(0, H)], m_send.at[0], m_recv.at[0, 1])
     plane_sent(stage, rows, H + 1, p_send, p_recv)
     plane_sent(ysend, yrecv, H + 1, y_send, y_recv)
     plane_wait(ysend, yrecv, H + 1, y_send, y_recv)
@@ -423,9 +429,8 @@
             v = v + rin[direction, 0, q].astype(F32)
         out[q] = v.astype(BF)
         out_copy(q).start()
+    all_sent(rout.at[:, 0, :, pl.ds(0, caps[1])], r_send.at[0], r_recv.at[0, 0, 0])
     for q in range(Q):
-        for direction in range(2):
-            r_copy(direction, 1, q).wait_send()
         out_copy(q).wait()
 
 
@@ -481,15 +486,15 @@
             dma((7,)),
             dma((Q,)),
             dma((3, Q)),
+            dma((1,)),
             dma((2, H + 1)),
-            dma((2, H + 1)),
+            dma((H,)),
             dma((2, H, Q)),
-            dma((2, H, Q)),
-            dma((H + 1, PL)),
-            dma((H + 1, PL)),
-            dma((H + 1, PL)),
-            dma((H + 1, PL)),
-            dma((2, H, Q)),
+            dma((H + 1,)),
+            dma((H + 1,)),
+            dma((H + 1,)),
+            dma((H + 1,)),
+            dma((H,)),
             dma((2, H, Q)),
         ],
         compiler_params=pltpu.CompilerParams(

time: 189 us -> 186 us (0.984)
  Pallas kernels: 187 us -> 184 us
    pallas_call x1, Pallas kernels: 187 us -> 184 us  [body(): pl.pallas_call(functools.partial(kernel, dm), out_shape=jax.ShapeDtypeStr...]
where the time goes in v6:
time: 186 us
  Pallas kernels  184 us (99%)
  local copies, waits for them, and re-layouts  1.88 us (1%)
    pallas_call x1, Pallas kernels, body(): pl.pallas_call(functools.partial(kernel, dm), out_shape=jax.ShapeDtypeStr...  184 us

profile of v6, /device:TPU:33, one launch (start us, length us, event | category | flops | bytes accessed | tf_op | source)
XLA Modules:
  0.0 185.6 jit_solution(18363080031084387241)
XLA Ops:
  0.0 183.7 %routed_experts.1 = bf16[128,2048]{1,0:T(8,128)(2,1)} custom-call(bf16[128,2048]{1,0:T(8,128)(2,1)} %hid_in.1, s32[2,128]{1,0:T(2,128)} %bitcast.4, f32[2,128]{1,0:T(2,128)} %bitcast.5, f32[1,2048]{1,0:T(1,128)} %bitcast.3, bf16[1,2048,512]{2,1,0:T(8,128)(2,1)} %wg.1, bf16[1,2048,512]{2,1,0:T(8,128)(2,1)} %wu.1, bf16[1,512,2048]{2,1,0:T(8,128)(2,1)} %wd.1), custom_call_target="tpu_custom_call" | custom-call | tf_op jit(solution)/shard_map/routed_experts/pallas_call | solution.py:448
  183.7 1.9 %copy.9 = bf16[128,2048]{1,0:T(8,128)(2,1)} copy(bf16[128,2048]{1,0:T(8,128)(2,1)} %routed_experts.1) | data formatting | bytes 1048576

commit v7 on v6

--- a/solution.py
+++ b/solution.py
@@ -44,7 +44,7 @@
     dm, hid_in, ids_in, wts_in, gain_in, wg, wu, wd, out_ref,
     hid, idv, wtv, gain, out,
     xs, metas, zb, zp, rin, rout, stage, rows, ysend, yrecv,
-    ex, cm, sm, st, erow, upper, perm_g, perm_s, acc, xb, gacc, uacc, hb, yb,
+    ex, cm, sm, st, e_all, c_all, erow, upper, perm_g, perm_s, acc, xb, gacc, uacc, hb, yb,
     wgv, wuv, wdv,
     i_sem, o_sem, w_sem, m_send, m_recv, z_send, z_recv, p_send, p_recv, y_send, y_recv, r_send, r_recv,
 ):
@@ -163,8 +163,10 @@
 
     others = pl.ds(1, PL - 1)
 
+    peers = sorted(range(1, PL), key=lambda j: -min(j % NX, NX - j % NX))
+
     def plane_start(src, dst, t, send, recv):
-        for j in range(1, PL):
+        for j in peers:
             plane_copy(src, dst, t, j, mirror(j), send, recv).start()
 
     def plane_wait(src, dst, t, send, recv):
@@ -234,6 +236,25 @@
     def only_q_cols(v, q):
         return jnp.where(q_col == q, v.astype(F32), 0.0).astype(BF)
 
+    cH = caps[H]
+    n_all = 2 * Q * cH
+
+    def build_last():
+        r_ax, n_ax = lax.broadcasted_iota(I32, (T, n_all), 0), lax.broadcasted_iota(I32, (T, n_all), 1)
+        e_sum = jnp.zeros((NR, n_all), F32)
+        for direction in range(2):
+            spread = jnp.where((n_ax % cH == r_ax) & (n_ax // (Q * cH) == direction), 1.0, 0.0).astype(BF)
+            e_sum = e_sum + mm(ex[direction, H], spread)
+        q_n = (lax.broadcasted_iota(I32, (1, n_all), 1) // cH) % Q
+        e_all[...] = jnp.where(q_row == q_n, e_sum, 0.0).astype(BF)
+        n_ax, r_ax = lax.broadcasted_iota(I32, (n_all, T), 0), lax.broadcasted_iota(I32, (n_all, T), 1)
+        c_sum = jnp.zeros((n_all, NR), F32)
+        for direction in range(2):
+            spread = jnp.where((n_ax % cH == r_ax) & (n_ax // (Q * cH) == direction), 1.0, 0.0).astype(BF)
+            c_sum = c_sum + mm(spread, cm[direction, H])
+        q_n = (lax.broadcasted_iota(I32, (n_all, 1), 0) // cH) % Q
+        c_all[...] = jnp.where(q_n == q_col, c_sum, 0.0).astype(BF)
+
     def own_block():
         build(0, 0)
         acc[0] = jnp.zeros((NR, DQ), F32)
@@ -293,6 +314,19 @@
         lax.fori_loop(0, 2 * Q, one, 0)
         scatter(k0, then)
 
+    def dispatch_last():
+        def arrived(i, _):
+            q, direction = i // 2, i % 2
+            z_copy(zb.at[direction, H - 1, q, pl.ds(0, cH)], direction, H, q, cH).wait_recv()
+            return 0
+
+        lax.fori_loop(0, 2 * Q, arrived, 0)
+        data = zb[:, H - 1, :, pl.ds(0, cH), :].reshape(n_all, DQ)
+        v = mm(e_all[...], data).astype(BF).reshape(PL, RB, DQ)
+        stage[H - 1, :, 0] = v
+        rows[H - 1, 0, 0] = v[0]
+        plane_start(stage, rows, H, p_send, p_recv)
+
     def dispatch(k, beside):
         ck = caps[k]
         acc[...] = jnp.zeros_like(acc)
@@ -306,26 +340,24 @@
                         relay_meta(direction, relay_at[k, at_q])
             z_copy(zb.at[direction, k - 1, q, pl.ds(0, ck)], direction, k, q, ck).wait_recv()
             data = zb[direction, k - 1, q, pl.ds(0, ck), :]
-            if k < H:
-                cn = caps[k + 1]
-                if k + 1 >= KP:
-                    p = k + 1 - KP
-                    zp[direction, p, q, pl.ds(0, cn), :] = mm(sm[direction, k][:cn, :ck], data).astype(BF)
-                    source = zp.at[direction, p, q, pl.ds(0, cn)]
-                else:
-                    source = zb.at[direction, k - 1, q, pl.ds(0, cn)]
-                z_copy(source, direction, k + 1, q, cn).start()
+            cn = caps[k + 1]
+            if k + 1 >= KP:
+                p = k + 1 - KP
+                zp[direction, p, q, pl.ds(0, cn), :] = mm(sm[direction, k][:cn, :ck], data).astype(BF)
+                source = zp.at[direction, p, q, pl.ds(0, cn)]
+            else:
+                source = zb.at[direction, k - 1, q, pl.ds(0, cn)]
+            z_copy(source, direction, k + 1, q, cn).start()
             e = only_q_rows(ex[direction, k], q)
             if ck < T:
                 e = e[:, :ck]
-            block = direction if k < H else 0
-            acc[block] = acc[block] + mm(e, data)
+            acc[direction] = acc[direction] + mm(e, data)
             if beside:
                 piece(i)
             return 0
 
         lax.fori_loop(0, 2 * Q, chunk, 0)
-        for block in range(2 if k < H else 1):
+        for block in range(2):
             v = acc[block].astype(BF).reshape(PL, RB, DQ)
             stage[k - 1, :, block] = v
             rows[k - 1, 0, block] = v[0]
@@ -354,19 +386,26 @@
     build_steps(1, 2)
     dispatch(1, False)
     build_steps(2, min(3, H + 1))
+    if H == 2:
+        build_last()
     for copy in weight_copies:
         copy.wait()
     builds_after = {2: (3, 4), 3: (4, 5), 4: (5, 7), 5: (7, 8), 7: (8, 9)}
     for k in range(2, H + 1):
         if k in beside:
             gather(beside[k])
-        dispatch(k, k in beside)
+        if k == H:
+            dispatch_last()
+        else:
+            dispatch(k, k in beside)
         if k in beside and k < KP:
             scatter(beside[k], send_results)
             sent.append(beside[k])
         lo, hi = builds_after.get(k, (H + 1, H + 1))
         if lo <= H:
             build_steps(lo, min(hi, H + 1))
+            if lo <= H < hi:
+                build_last()
     late = [k0 for k0 in beside.values() if k0 not in sent]
     for k0 in late:
         scatter(k0)
@@ -390,12 +429,15 @@
         ck = caps[k]
         plane_wait(ysend, yrecv, k, y_send, y_recv)
 
+        if k == H:
+            v = mm(c_all[...], yrecv[H - 1, :, 0].reshape(NR, DQ)).astype(BF)
+            rout[:, H - 1, :, pl.ds(0, cH), :] = v.reshape(2, Q, cH, DQ)
+
         def back(i, _, k=k, ck=ck):
             q, direction = i // 2, i % 2
-            block = direction if k < H else 0
-            y = yrecv[k - 1, :, block].reshape(NR, DQ)
-            v = mm(only_q_cols(cm[direction, k, pl.ds(0, ck), :], q), y)
             if k < H:
+                y = yrecv[k - 1, :, direction].reshape(NR, DQ)
+                v = mm(only_q_cols(cm[direction, k, pl.ds(0, ck), :], q), y)
                 cn = caps[k + 1]
                 r_copy(direction, k + 1, q).wait_recv()
                 far = rin[direction, k, q, pl.ds(0, cn), :]
@@ -403,7 +445,7 @@
                     v = v + mm(st[direction, k][:ck, :cn], far)
                 else:
                     v = v + far.astype(F32)
-            rout[direction, k - 1, q, pl.ds(0, ck), :] = v.astype(BF)
+                rout[direction, k - 1, q, pl.ds(0, ck), :] = v.astype(BF)
             r_copy(direction, k, q).start()
             return 0
 
@@ -470,6 +512,8 @@
             vm((2, H + 1, T, NR), BF),
             vm((2, H + 1, T, T), BF),
             vm((2, H + 1, T, T), BF),
+            vm((NR, 2 * Q * dm.caps[H]), BF),
+            vm((2 * Q * dm.caps[H], NR), BF),
             vm((NR, T), I32),
             vm((T, T), BF),
             vm((Q * SR, Q * SR), BF),

time: 186 us -> 186 us (level)
  no operation moved by 1% of the time
where the time goes in v7:
time: 186 us
  Pallas kernels  184 us (99%)
  local copies, waits for them, and re-layouts  1.88 us (1%)
    pallas_call x1, Pallas kernels, body(): pl.pallas_call(functools.partial(kernel, dm), out_shape=jax.ShapeDtypeStr...  184 us

profile of v7, /device:TPU:33, one launch (start us, length us, event | category | flops | bytes accessed | tf_op | source)
XLA Modules:
  0.0 185.9 jit_solution(17800816841722482154)
XLA Ops:
  0.0 184.0 %routed_experts.1 = bf16[128,2048]{1,0:T(8,128)(2,1)} custom-call(bf16[128,2048]{1,0:T(8,128)(2,1)} %hid_in.1, s32[2,128]{1,0:T(2,128)} %bitcast.4, f32[2,128]{1,0:T(2,128)} %bitcast.5, f32[1,2048]{1,0:T(1,128)} %bitcast.3, bf16[1,2048,512]{2,1,0:T(8,128)(2,1)} %wg.1, bf16[1,2048,512]{2,1,0:T(8,128)(2,1)} %wu.1, bf16[1,512,2048]{2,1,0:T(8,128)(2,1)} %wd.1), custom_call_target="tpu_custom_call" | custom-call | tf_op jit(solution)/shard_map/routed_experts/pallas_call | solution.py:490
  184.0 1.9 %copy.9 = bf16[128,2048]{1,0:T(8,128)(2,1)} copy(bf16[128,2048]{1,0:T(8,128)(2,1)} %routed_experts.1) | data formatting | bytes 1048576

commit v8 on v7

--- a/solution.py
+++ b/solution.py
@@ -163,10 +163,8 @@
 
     others = pl.ds(1, PL - 1)
 
-    peers = sorted(range(1, PL), key=lambda j: -min(j % NX, NX - j % NX))
-
     def plane_start(src, dst, t, send, recv):
-        for j in peers:
+        for j in range(1, PL):
             plane_copy(src, dst, t, j, mirror(j), send, recv).start()
 
     def plane_wait(src, dst, t, send, recv):
@@ -421,7 +419,8 @@
         return pltpu.make_async_remote_copy(
             src_ref=rout.at[direction, k - 1, q, pl.ds(0, caps[k])],
             dst_ref=rin.at[direction, k - 1, q, pl.ds(0, caps[k])],
-            send_sem=r_send.at[k - 1], recv_sem=r_recv.at[direction, k - 1, q],
+            send_sem=r_send.at[k - 1],
+            recv_sem=z_recv.at[direction, k - 1, q] if k < H else r_recv.at[direction, q],
             device_id=backward(direction), device_id_type=MESH,
         )
 
@@ -454,7 +453,7 @@
         plane_sent(ysend, yrecv, k, y_send, y_recv)
         all_sent(zb.at[:, k - 1, :, pl.ds(0, ck)], z_send.at[k - 1], z_recv.at[0, k - 1, 0])
         if k < H:
-            all_sent(rout.at[:, k, :, pl.ds(0, caps[k + 1])], r_send.at[k], r_recv.at[0, k, 0])
+            all_sent(rout.at[:, k, :, pl.ds(0, caps[k + 1])], r_send.at[k], r_recv.at[0, 0])
     all_sent(metas.at[:, pl.ds(0, H)], m_send.at[0], m_recv.at[0, 1])
     plane_sent(stage, rows, H + 1, p_send, p_recv)
     plane_sent(ysend, yrecv, H + 1, y_send, y_recv)
@@ -471,7 +470,7 @@
             v = v + rin[direction, 0, q].astype(F32)
         out[q] = v.astype(BF)
         out_copy(q).start()
-    all_sent(rout.at[:, 0, :, pl.ds(0, caps[1])], r_send.at[0], r_recv.at[0, 0, 0])
+    all_sent(rout.at[:, 0, :, pl.ds(0, caps[1])], r_send.at[0], r_recv.at[0, 0])
     for q in range(Q):
         out_copy(q).wait()
 
@@ -539,7 +538,7 @@
             dma((H + 1,)),
             dma((H + 1,)),
             dma((H,)),
-            dma((2, H, Q)),
+            dma((2, Q)),
         ],
         compiler_params=pltpu.CompilerParams(
             collective_id=0, has_side_effects=True, vmem_limit_bytes=66 * 1000 * 1000

time: 186 us -> 185 us (level)
  no operation moved by 1% of the time
where the time goes in v8:
time: 185 us
  Pallas kernels  183 us (99%)
  local copies, waits for them, and re-layouts  1.88 us (1%)
    pallas_call x1, Pallas kernels, body(): pl.pallas_call(functools.partial(kernel, dm), out_shape=jax.ShapeDtypeStr...  183 us

profile of v8, /device:TPU:33, one launch (start us, length us, event | category | flops | bytes accessed | tf_op | source)
XLA Modules:
  0.0 185.1 jit_solution(15022777949866529565)
XLA Ops:
  0.0 183.2 %routed_experts.1 = bf16[128,2048]{1,0:T(8,128)(2,1)} custom-call(bf16[128,2048]{1,0:T(8,128)(2,1)} %hid_in.1, s32[2,128]{1,0:T(2,128)} %bitcast.4, f32[2,128]{1,0:T(2,128)} %bitcast.5, f32[1,2048]{1,0:T(1,128)} %bitcast.3, bf16[1,2048,512]{2,1,0:T(8,128)(2,1)} %wg.1, bf16[1,2048,512]{2,1,0:T(8,128)(2,1)} %wu.1, bf16[1,512,2048]{2,1,0:T(8,128)(2,1)} %wd.1), custom_call_target="tpu_custom_call" | custom-call | tf_op jit(solution)/shard_map/routed_experts/pallas_call | solution.py:489
  183.2 1.9 %copy.9 = bf16[128,2048]{1,0:T(8,128)(2,1)} copy(bf16[128,2048]{1,0:T(8,128)(2,1)} %routed_experts.1) | data formatting | bytes 1048576
